TPU v7x, 512 devices: a whole 4x8x8 slice. The times are simulated.
512 devices in a mesh: ep: 32 (over z, x), tp: 16 (over y, core).
Axes of the slice: x: 4, y: 8, z: 8, core: 2. Of those that a mesh axis runs over, the one named last changes fastest.
Arguments:
- queries: bfloat16 [196608, 1024], P(('ep', 'tp')), may hold values from -250 to 250
- keys_values: bfloat16 [2, 196608, 256], P(None, ('ep', 'tp')), may hold values from -8 to 8
- sink_logits: float32 [16], replicated, may hold values from 2 to 6
- moe_rows: bfloat16 [8192, 2048], P('ep'), may hold values from -600 to 600
- norm_gain: float32 [2048], replicated, may hold values from 0.1 to 1.9
- group_choice: int32 [8192], P('ep'), may hold values from 0 to 7, as said below
- member_choice: int32 [8192, 2], P('ep'), may hold values from 0 to 3, as said below
- route_weight: float32 [8192, 2], P('ep'), may hold values from 0.1 to 1
- w_gate: bfloat16 [32, 2048, 2048], P('ep', None, 'tp'), may hold values from -0.125 to 0.125
- w_up: bfloat16 [32, 2048, 2048], P('ep', None, 'tp'), may hold values from -0.125 to 0.125
- w_down: bfloat16 [32, 2048, 2048], P('ep', None, 'tp'), may hold values from -0.125 to 0.125
Outputs:
- attended: bfloat16 [196608, 1024], P(('ep', 'tp'))
- mixed: bfloat16 [8192, 2048], P('ep', 'tp')
Inputs may be any that keep to these rules, and one draw needn't show every extreme that they name: With expert = group_choice * 4 + member_choice, within the 256 rows of one index of ep no expert is named by more than 32 rows, and some expert is named by exactly 32 rows. `member_choice`: the 2 entries of a row differ.
All inputs are finite; a program needn't handle non-finite values.
Results may differ from a plain program's by a relative error of at most 0.007.
Values may be sent and summed in bfloat16 or wider, within the bound.
No kernel may reach another device: no remote copies, remote signals or barrier semaphores. Data moves between devices by JAX's collectives and lax.ppermute only.
A program may use at most 64 MiB of HBM per device.

v0:
```python
import jax
import jax.numpy as jnp
from jax import lax
from jax.sharding import PartitionSpec as P

QH = 16
KVH = 4
HD = 64
WINDOW = 128
EPG = 4
TOP = 2


def passed_along(value, axis, by):
    peers = lax.axis_size(axis)
    pairs = [(i, i + by) for i in range(peers) if 0 <= i + by < peers]
    return lax.ppermute(value, axis, pairs)


def attend_window(queries, keys_values, sink_logits):
    length = queries.shape[0]
    sharing = QH // KVH
    blocks = length // WINDOW
    edge_rows = keys_values[:, length - WINDOW :, :]
    earlier_keys = passed_along(edge_rows, ("ep", "tp"), 1)
    joined = jnp.concatenate([earlier_keys, keys_values], axis=1)
    first_half = joined[:, :length].reshape(2, blocks, WINDOW, KVH, HD)
    second_half = joined[:, WINDOW:].reshape(2, blocks, WINDOW, KVH, HD)
    banded = jnp.concatenate([first_half, second_half], axis=2)
    query_blocks = queries.reshape(blocks, WINDOW, KVH, sharing, HD)
    scores = jnp.einsum(
        "bqhgd,bkhd->bhgqk", query_blocks, banded[0], preferred_element_type=jnp.float32
    ) * HD ** (-0.5)
    offset = lax.axis_index(("ep", "tp")) * length
    key_column = jnp.arange(2 * WINDOW, dtype=jnp.int32)
    distance = jnp.arange(WINDOW, dtype=jnp.int32)[:, None] + WINDOW - key_column[None, :]
    inside = (distance >= 0) & (distance < WINDOW)
    key_position = (
        offset
        + jnp.arange(blocks, dtype=jnp.int32)[:, None] * WINDOW
        + key_column[None, :]
        - WINDOW
    )
    visible = inside[None, :, :] & (key_position[:, None, :] >= 0)
    scores = jnp.where(visible[:, None, None, :, :], scores, -1e30)
    sink_column = sink_logits.reshape(KVH, sharing)[None, :, :, None]
    highest = jnp.maximum(jnp.max(scores, axis=-1), sink_column)
    weights = jnp.exp(scores - highest[..., None])
    totals = jnp.sum(weights, axis=-1) + jnp.exp(sink_column - highest)
    summed = jnp.einsum(
        "bhgqk,bkhd->bqhgd",
        weights.astype(jnp.bfloat16),
        banded[1],
        preferred_element_type=jnp.float32,
    )
    attended = summed / jnp.transpose(totals, (0, 3, 1, 2))[..., None]
    return attended.astype(jnp.bfloat16).reshape(length, QH * HD)


def route_experts(
    moe_rows, norm_gain, group_choice, member_choice, route_weight, w_gate, w_up, w_down
):
    token_count = moe_rows.shape[0]
    row_width = moe_rows.shape[1]
    ep_count = lax.axis_size("ep")
    local_experts = w_gate.shape[0]
    expert_count = ep_count * local_experts
    capacity = 2 * TOP * token_count // expert_count
    values = moe_rows.astype(jnp.float32)
    normed = (
        values * lax.rsqrt(jnp.mean(values * values, axis=1, keepdims=True) + 1e-06) * norm_gain
    ).astype(jnp.bfloat16)
    chosen = (group_choice[:, None] * EPG + member_choice).reshape(-1)
    onehot = (chosen[:, None] == jnp.arange(expert_count, dtype=jnp.int32)[None, :]).astype(
        jnp.int32
    )
    earlier = jnp.cumsum(onehot, axis=0) - onehot
    destination = chosen * capacity + jnp.sum(earlier * onehot, axis=1)
    source_row = jnp.arange(token_count * TOP, dtype=jnp.int32) // TOP
    lookup = (
        jnp.full((expert_count * capacity,), token_count, jnp.int32).at[destination].set(source_row)
    )
    padded = jnp.concatenate([normed, jnp.zeros((1, row_width), jnp.bfloat16)], axis=0)
    share_count = capacity // lax.axis_size("tp")
    slot_table = lookup.reshape(expert_count, capacity)
    my_slots = lax.dynamic_slice_in_dim(
        slot_table, lax.axis_index("tp") * share_count, share_count, 1
    )
    outgoing = padded[my_slots.reshape(-1)].reshape(ep_count, local_experts, share_count, row_width)
    incoming = lax.all_to_all(outgoing, "ep", split_axis=0, concat_axis=0, tiled=True)
    block_rows = lax.all_gather(incoming, "tp", axis=2, tiled=True)
    gate_part = jnp.einsum("secd,edf->secf", block_rows, w_gate, preferred_element_type=jnp.float32)
    up_part = jnp.einsum("secd,edf->secf", block_rows, w_up, preferred_element_type=jnp.float32)
    hidden = (jax.nn.silu(gate_part) * up_part).astype(jnp.bfloat16)
    out_width = w_down.shape[2]
    produced = jnp.einsum(
        "secf,efd->secd",
        lax.all_gather(hidden, "tp", axis=3, tiled=True),
        w_down,
        preferred_element_type=jnp.float32,
    )
    produced = produced.astype(jnp.bfloat16).reshape(ep_count, local_experts * capacity, out_width)
    returned = lax.all_to_all(produced, "ep", split_axis=0, concat_axis=0, tiled=True)
    picked = returned.reshape(expert_count * capacity, out_width)[destination]
    picked = picked.reshape(token_count, TOP, out_width).astype(jnp.float32)
    return jnp.sum(route_weight[:, :, None] * picked, axis=1).astype(jnp.bfloat16)


def shards(
    queries,
    keys_values,
    sink_logits,
    moe_rows,
    norm_gain,
    group_choice,
    member_choice,
    route_weight,
    w_gate,
    w_up,
    w_down,
):
    attended = attend_window(queries, keys_values, sink_logits)
    mixed = route_experts(
        moe_rows, norm_gain, group_choice, member_choice, route_weight, w_gate, w_up, w_down
    )
    return (attended, mixed)


def solution(mesh):
    in_specs = (
        P(("ep", "tp"), None),
        P(None, ("ep", "tp"), None),
        P(),
        P("ep", None),
        P(),
        P("ep"),
        P("ep", None),
        P("ep", None),
        P("ep", None, "tp"),
        P("ep", None, "tp"),
        P("ep", None, "tp"),
    )
    out_specs = (P(("ep", "tp"), None), P("ep", "tp"))
    return jax.shard_map(shards, mesh=mesh, in_specs=in_specs, out_specs=out_specs, check_vma=False)
```

profile of v0, /device:TPU:8, one launch (start us, length us, event | category | flops | bytes accessed | tf_op | source)
XLA Modules:
  0.0 180.2 jit_solution(10579058305532520949)
XLA Ops:
  7.2 0.7 broadcast_multiply_fusion.1
  8.0 0.7 broadcast_multiply_fusion
  8.6 0.1 copy.40
  8.8 0.1 eq.29
  8.9 0.1 eq.25
  9.1 1.2 reduce-window.6
  10.3 0.2 slice_reduce_fusion
  10.5 0.1 copy.39
  10.7 0.1 mul.102
  10.8 0.1 fusion.55
  11.0 2.4 %scatter_custom_fusion = s32[1024]{0:T(1024)S(1)} fusion(s32[512]{0:T(512)S(1)} %bitcast.107, s32[512]{0:T(512)S(1)} %add_select_fusion, s32[]{:T(128)} %constant.66.clone.1), kind=kCustom, calls=%fused_computation.75 | custom fusion | bytes 4100 | tf_op jit(solution)/shard_map/scatter | solution.py:81
  13.5 0.1 constant_dynamic-slice_fusion
  13.6 0.1 reshape.204
  13.7 1.5 fusion.17
  15.2 1.5 fusion.19
  16.7 0.1 concatenate.11
  16.8 0.7 gather_fusion
  17.6 0.2 reshape.205
  17.8 25.9 %all_to_all.10 = bf16[32,1,2,2048]{3,2,1,0:T(2,128)(2,1)S(1)} all-to-all(bf16[32,1,2,2048]{3,2,1,0:T(2,128)(2,1)S(1)} %bitcast.105), channel_id=1, replica_groups=mesh['ep'=32,'tp'=16] {'ep'}, dimensions={0} | all-to-all | bytes 524288 | tf_op jit(solution)/shard_map/all_to_all | solution.py:90
  43.7 0.8 copy.44
  44.6 39.7 %all-gather.3.cloned.1.call-done = bf16[32,1,32,2048]{3,0,1,2:T(8,128)(2,1)} async-done(((bf16[32,1,2,2048]{3,0,1,2:T(8,128)(2,1)}), bf16[32,1,32,2048]{3,0,1,2:T(8,128)(2,1)}) %all-gather.3.cloned.1.call-update) | async-done | bytes 4194320 | tf_op jit(solution)/shard_map/all_gather | solution.py:91
  84.2 5.2 %fusion.25 = f32[32,1,32,128]{3,2,0,1:T(8,128)S(1)} fusion(bf16[32,1,32,2048]{3,0,1,2:T(8,128)(2,1)} %all-gather.3.cloned.1.call-done, bf16[1,2048,128]{2,1,0:T(8,128)(2,1)S(1)} %copy-done), kind=kOutput, calls=%fused_computation.30 | convolution fusion | flops 536870912 | bytes 5242880 | tf_op jit(solution)/shard_map/secd,edf->secf/dot_general | solution.py:92
  89.5 3.6 %fusion.34 = bf16[32,1,32,128]{3,2,0,1:T(8,128)(2,1)} fusion(bf16[32,1,32,2048]{3,0,1,2:T(8,128)(2,1)S(1)} %copy-done.6, bf16[1,2048,128]{2,1,0:T(8,128)(2,1)S(1)} %copy-done.7, f32[32,1,32,128]{3,2,0,1:T(8,128)S(1)} %fusion.25), kind=kOutput, calls=%fused_computation.33 | convolution fusion | flops 537657344 | bytes 5505024 | tf_op jit(solution)/shard_map/secd,edf->secf/dot_general | solution.py:93
  93.2 2.3 %collective-permute-start = (bf16[2,128,256]{2,1,0:T(8,128)(2,1)S(1)}, bf16[2,128,256]{2,1,0:T(8,128)(2,1)S(1)}, u32[]{:S(2)}, u32[]{:S(2)}) collective-permute-start(bf16[2,128,256]{2,1,0:T(8,128)(2,1)S(1)} %slice.18), channel_id=1, source_target_pairs={{0,1},{1,2},{2,3},{3,4},{4,5},{5,6},{6,7},{7,8},{8,9},{9,10},{10,1... | collective-permute-start | bytes 393224 | tf_op jit(solution)/shard_map/ppermute | solution.py:17
  95.5 0.1 add_compare_fusion
  95.6 0.2 broadcast_and_fusion
  95.8 0.3 reshape.243
  96.1 0.5 copy.33
  96.6 3.4 %reshape.244 = bf16[3,128,4,4,64]{4,3,2,1,0:T(4,128)(2,1)S(1)} reshape(bf16[384,1024]{1,0:T(8,128)(2,1)} %param.11) | data formatting | bytes 1572864 | tf_op jit(solution)/shard_map/reshape | solution.py:30
  100.0 0.1 max.16
  100.1 0.1 copy.38
  100.2 0.8 pad_maximum_fusion.1
  101.0 1.8 %reshape.242 = bf16[2,3,128,4,64]{4,3,2,1,0:T(4,128)(2,1)S(1)} reshape(bf16[2,384,256]{2,1,0:T(8,128)(2,1)} %pad_maximum_fusion.1) | data formatting | bytes 786432 | tf_op jit(solution)/shard_map/reshape | solution.py:27
  102.8 1.1 copy.32
  103.9 2.2 %fusion.2 = (f32[3,4,4,128]{3,2,1,0:T(4,128)S(1)}, f32[3,4,256,128,4]{3,2,4,1,0:T(8,128)S(1)}) fusion(pred[3,128,256]{1,2,0:T(8,128)(4,1)S(1)} %broadcast_and_fusion, bf16[3,128,4,4,64]{4,3,2,1,0:T(4,128)(2,1)S(1)} %reshape.244, bf16[2,3,128,4,64]{2,4,3,1,0:T(8,128)(2,1)S(1)} %copy.33, bf16[2,3,128,4,64]{2,4,3,1,0:T(8,128)(2,1)} %copy.32), kind=kOutput, calls=%fused_computation.7 | convolution fusion | flops 206825472 | bytes 7987200 | tf_op jit(solution)/shard_map/bqhgd,bkhd->bhgqk/dot_general | solution.py:31
  106.2 0.1 broadcast_maximum_fusion
  106.3 2.6 %copy-done.1 = f32[3,4,256,128,4]{3,2,4,1,0:T(8,128)} copy-done((f32[3,4,256,128,4]{3,2,4,1,0:T(8,128)}, f32[3,4,256,128,4]{3,2,4,1,0:T(8,128)S(1)}, u32[]{:S(2)}) %copy-start.1) | copy-done | bytes 6291480
  108.9 1.6 fusion
  110.5 0.1 add_bitcast_fusion.1
  110.6 32.6 %all-gather.5.cloned.1.call-done = bf16[32,1,32,2048]{3,2,0,1:T(8,128)(2,1)} async-done(((bf16[32,1,32,128]{3,2,0,1:T(8,128)(2,1)}), bf16[32,1,32,2048]{3,2,0,1:T(8,128)(2,1)}) %all-gather.5.cloned.1.call-update) | async-done | bytes 4194320 | tf_op jit(solution)/shard_map/all_gather | solution.py:98
  143.2 4.2 %fusion.37 = bf16[32,32,128]{2,1,0:T(8,128)(2,1)} fusion(bf16[32,1,32,2048]{3,2,0,1:T(8,128)(2,1)} %all-gather.5.cloned.1.call-done, bf16[1,2048,128]{2,1,0:T(8,128)(2,1)S(1)} %copy-done.8), kind=kOutput, calls=%fused_computation.34 | convolution fusion | flops 537001984 | bytes 4980736 | tf_op jit(solution)/shard_map/secf,efd->secd/dot_general | solution.py:96
  147.4 10.2 %all-to-all-start.1 = ((bf16[32,32,128]{2,1,0:T(8,128)(2,1)}), bf16[32,32,128]{2,1,0:T(8,128)(2,1)S(1)}, u32[]{:S(2)}, u32[]{:S(2)}) async-start(bf16[32,32,128]{2,1,0:T(8,128)(2,1)} %fusion.37), calls=%async_computation.1 | async-start | bytes 524288 | tf_op jit(solution)/shard_map/all_to_all | solution.py:103
  157.6 5.2 %fusion.20 = bf16[3,128,4,4,64]{1,4,3,2,0:T(8,128)(2,1)} fusion(f32[3,4,256,128,4]{3,2,4,1,0:T(8,128)} %copy-done.1, f32[3,4,4,128]{3,2,1,0:T(4,128)S(1)} %broadcast_maximum_fusion, pred[3,128,256]{1,2,0:T(8,128)(4,1)S(1)} %broadcast_and_fusion, f32[3,128,4,4]{1,3,2,0:T(4,128)S(1)} %add_bitcast_fusion.1, bf16[2,3,128,4,64]{2,4,3,1,0:T(8,128)(2,1)S(1)} %copy-done.3, ...), kind=kOutput, calls=%fused_computation.27 | convolution fusion | flops 209190912 | bytes 8011776 | tf_op jit(solution)/shard_map/bhgqk,bkhd->bqhgd/dot_general | solution.py:50
  162.8 2.8 %copy.56 = bf16[3,128,4,4,64]{4,3,2,1,0:T(4,128)(2,1)S(1)} copy(bf16[3,128,4,4,64]{1,4,3,2,0:T(8,128)(2,1)} %fusion.20) | data formatting | bytes 1572864
  165.6 1.9 %reshape.245 = bf16[384,1024]{1,0:T(8,128)(2,1)} reshape(bf16[3,128,4,4,64]{4,3,2,1,0:T(4,128)(2,1)S(1)} %copy.56) | data formatting | bytes 1572864
  167.4 3.5 %all-to-all-done.1 = bf16[32,32,128]{2,1,0:T(8,128)(2,1)S(1)} async-done(((bf16[32,32,128]{2,1,0:T(8,128)(2,1)}), bf16[32,32,128]{2,1,0:T(8,128)(2,1)S(1)}, u32[]{:S(2)}, u32[]{:S(2)}) %all-to-all-start.1) | async-done | bytes 262176 | tf_op jit(solution)/shard_map/all_to_all | solution.py:103
  170.9 1.3 gather_fusion.1
  172.3 1.1 fusion.49
  (36 shorter events, 0.4 us)
Async XLA Ops:
  7.2 77.1 %copy-start = (bf16[1,2048,128]{2,1,0:T(8,128)(2,1)S(1)}, bf16[1,2048,128]{2,1,0:T(8,128)(2,1)}, u32[]{:S(2)}) copy-start(bf16[1,2048,128]{2,1,0:T(8,128)(2,1)} %param.19) | copy-start | bytes 1572868
  7.2 77.1 %all-gather.3.cloned.1.call-start = ((), (), s32[]{:S(2)}) async-start(), calls=%async_computation.2 | async-start | bytes 4456448 | tf_op jit(solution)/shard_map/all_gather | solution.py:91
  17.8 71.7 %copy-start.7 = (bf16[1,2048,128]{2,1,0:T(8,128)(2,1)S(1)}, bf16[1,2048,128]{2,1,0:T(8,128)(2,1)}, u32[]{:S(2)}) copy-start(bf16[1,2048,128]{2,1,0:T(8,128)(2,1)} %param.20) | copy-start | bytes 1572868
  44.5 98.7 %all-gather.5.cloned.1.call-start = ((), (), s32[]{:S(2)}) async-start(), calls=%async_computation.3 | async-start | bytes 4456448 | tf_op jit(solution)/shard_map/all_gather | solution.py:98
  84.2 5.2 %copy-start.6 = (bf16[32,1,32,2048]{3,0,1,2:T(8,128)(2,1)S(1)}, bf16[32,1,32,2048]{3,0,1,2:T(8,128)(2,1)}, u32[]{:S(2)}) copy-start(bf16[32,1,32,2048]{3,0,1,2:T(8,128)(2,1)} %all-gather.3.cloned.1.call-done) | copy-start | bytes 12582916
  89.5 3.7 %copy-start.2 = (bf16[2,384,256]{2,1,0:T(8,128)(2,1)S(1)}, bf16[2,384,256]{2,1,0:T(8,128)(2,1)}, u32[]{:S(2)}) copy-start(bf16[2,384,256]{2,1,0:T(8,128)(2,1)} %param.12) | copy-start | bytes 1179652
  93.1 6.9 %copy-start.5 = (f32[16]{0:T(128)S(1)}, f32[16]{0:T(128)}, u32[]{:S(2)}) copy-start(f32[16]{0:T(128)} %param.13) | copy-start | bytes 196
  93.1 7.0 %copy-start.4 = (f32[256,2]{0,1:T(2,128)S(1)}, f32[256,2]{0,1:T(2,128)}, u32[]{:S(2)}) copy-start(f32[256,2]{0,1:T(2,128)} %param.18) | copy-start | bytes 6148
  93.2 7.1 %collective-permute-start = (bf16[2,128,256]{2,1,0:T(8,128)(2,1)S(1)}, bf16[2,128,256]{2,1,0:T(8,128)(2,1)S(1)}, u32[]{:S(2)}, u32[]{:S(2)}) collective-permute-start(bf16[2,128,256]{2,1,0:T(8,128)(2,1)S(1)} %slice.18), channel_id=1, source_target_pairs={{0,1},{1,2},{2,3},{3,4},{4,5},{5,6},{6,7},{7,8},{8,9},{9,10},{10,1... | collective-permute-start | bytes 393224 | tf_op jit(solution)/shard_map/ppermute | solution.py:17
  106.2 2.7 %copy-start.1 = (f32[3,4,256,128,4]{3,2,4,1,0:T(8,128)}, f32[3,4,256,128,4]{3,2,4,1,0:T(8,128)S(1)}, u32[]{:S(2)}) copy-start(f32[3,4,256,128,4]{3,2,4,1,0:T(8,128)S(1)} %get-tuple-element.9) | copy-start | bytes 18874372
  106.2 37.0 %copy-start.8 = (bf16[1,2048,128]{2,1,0:T(8,128)(2,1)S(1)}, bf16[1,2048,128]{2,1,0:T(8,128)(2,1)}, u32[]{:S(2)}) copy-start(bf16[1,2048,128]{2,1,0:T(8,128)(2,1)} %param.21) | copy-start | bytes 1572868
  110.5 47.1 %copy-start.3 = (bf16[2,3,128,4,64]{2,4,3,1,0:T(8,128)(2,1)S(1)}, bf16[2,3,128,4,64]{2,4,3,1,0:T(8,128)(2,1)}, u32[]{:S(2)}) copy-start(bf16[2,3,128,4,64]{2,4,3,1,0:T(8,128)(2,1)} %copy.32) | copy-start | bytes 1179652
  147.4 23.6 %all-to-all-start.1 = ((bf16[32,32,128]{2,1,0:T(8,128)(2,1)}), bf16[32,32,128]{2,1,0:T(8,128)(2,1)S(1)}, u32[]{:S(2)}, u32[]{:S(2)}) async-start(bf16[32,32,128]{2,1,0:T(8,128)(2,1)} %fusion.37), calls=%async_computation.1 | async-start | bytes 524288 | tf_op jit(solution)/shard_map/all_to_all | solution.py:103
Sparse Core Ops, SparseCore 0:
  44.6 39.5 all-gather.2
  93.3 49.8 all-gather.4
where the time goes:
time: 181 us; the launch traced here: 180 us
  waiting for transfers between devices  75.8 us (42%)
  blocking collectives  25.9 us (14%)
  local copies, waits for them, and re-layouts  21.3 us (12%)
  matrix products  20.4 us (11%)
  between operations  14.4 us (8%)
  starting transfers between devices  12.6 us (7%)
  other arithmetic  9.73 us (5%)
    all_gather x1, waiting for transfers between devices, route_experts(): block_rows = lax.all_gather(incoming, 'tp', axis=2, tiled=True)  39.7 us
    all_gather x1, waiting for transfers between devices, route_experts(): lax.all_gather(hidden, 'tp', axis=3, tiled=True)  32.6 us
    all_to_all x1, blocking collectives, route_experts(): lax.all_to_all(outgoing, 'ep', split_axis=0, concat_axis=0, tiled=True)  25.9 us
    all_to_all x1, starting transfers between devices, route_experts(): lax.all_to_all(produced, 'ep', split_axis=0, concat_axis=0, tiled=True)  10.2 us
    unnamed x21, local copies, waits for them, and re-layouts  7.39 us
    dot_general x1, matrix products, attend_window(): jnp.einsum('bhgqk,bkhd->bqhgd', weights.astype(jnp.bfloat16), banded[1],...  5.22 us
    dot_general x1, matrix products, route_experts(): jnp.einsum('secd,edf->secf', block_rows, w_gate, preferred_element_type=j...  5.18 us
    dot_general x1, matrix products, route_experts(): jnp.einsum('secf,efd->secd', lax.all_gather(hidden, 'tp', axis=3, tiled=T...  4.15 us
  transfers between devices with their start and end apart: 4, of which 3 were waited for; matrix products, arithmetic and copies ran while one was open for 12% of the time, Pallas kernels for 0%

commit v1 on v0

v1 whole, which is shorter than its diff:
```python
import jax
import jax.numpy as jnp
from jax import lax
from jax.experimental import pallas as pl
from jax.experimental.pallas import tpu as pltpu
from jax.sharding import PartitionSpec as P

QH = 16
KVH = 4
HD = 64
WINDOW = 128
EPG = 4
TOP = 2
LANES = 128
ROW_SCALE = 256.0
EXP_LOW = -60
EXP_COUNT = 80


def attention_kernel(first_ref, sink_ref, q_ref, prev_ref, cur_ref, edge_ref, out_ref):
    block = pl.program_id(0)
    f32 = jnp.float32
    bf16 = jnp.bfloat16
    row = lax.broadcasted_iota(jnp.int32, (WINDOW, WINDOW), 0)
    col = lax.broadcasted_iota(jnp.int32, (WINDOW, WINDOW), 1)
    causal = col <= row
    lane = lax.broadcasted_iota(jnp.int32, (WINDOW, LANES), 1)
    low = lane < HD
    at_start = block == 0
    hidden_prev = jnp.where(at_start, first_ref[0], 0)
    floor = jnp.where(hidden_prev == 1, f32(-1e30), f32(0.0))
    keep = jnp.where(hidden_prev == 1, f32(0.0), f32(1.0))
    zero = jnp.zeros((WINDOW, LANES), bf16)
    for c in range(KVH):
        lanes = pl.ds((c // 2) * LANES, LANES)
        mine = low if c % 2 == 0 else jnp.logical_not(low)
        parts = []
        for which in range(2):
            before = jnp.where(at_start, edge_ref[which, :, lanes], prev_ref[which, :, lanes])
            now = cur_ref[which, :, lanes]
            halves = []
            for value in (before, now):
                own = jnp.where(mine, value, zero)
                swapped = pltpu.roll(own.astype(f32), HD, 1).astype(bf16)
                halves.append((own, swapped) if c % 2 == 0 else (swapped, own))
            (a_prev, b_prev), (a_cur, b_cur) = halves
            parts.append(jnp.concatenate([a_prev, a_cur, b_prev, b_cur], axis=0))
        keys, values = parts
        keys = keys * bf16(HD ** (-0.5))
        for p in range(2):
            head = c * 4 + p * 2
            at = c * 256 + p * LANES
            q = q_ref[:, at : at + LANES]
            scores = lax.dot_general(q, keys, (((1,), (1,)), ((), ())), preferred_element_type=f32)
            pieces = []
            sums = []
            for side in range(2):
                base = side * 2 * WINDOW
                s_prev = scores[:, base : base + WINDOW] * keep + floor
                s_cur = scores[:, base + WINDOW : base + 2 * WINDOW]
                s = jnp.where(causal, s_cur, s_prev)
                sink = sink_ref[head + side]
                highest = jnp.maximum(jnp.max(s, axis=1, keepdims=True), sink)
                w = jnp.exp(s - highest)
                sums.append(jnp.sum(w, axis=1, keepdims=True) + jnp.exp(sink - highest))
                rounded = w.astype(bf16)
                pieces.append(jnp.where(causal, zero, rounded))
                pieces.append(jnp.where(causal, rounded, zero))
            weights = jnp.concatenate(pieces, axis=1)
            summed = jnp.dot(weights, values, preferred_element_type=f32)
            total = jnp.where(low, sums[0], sums[1])
            out_ref[:, at : at + LANES] = (summed / total).astype(bf16)


def attend_window(queries, keys_values, sink_logits):
    length = queries.shape[0]
    blocks = length // WINDOW
    width = keys_values.shape[2]
    edge_rows = keys_values[:, length - WINDOW :, :]
    peers = lax.axis_size(("ep", "tp"))
    pairs = [(i, i + 1) for i in range(peers - 1)]
    edge = lax.ppermute(edge_rows, ("ep", "tp"), pairs)
    first = (lax.axis_index(("ep", "tp")) == 0).astype(jnp.int32).reshape(1)
    return pl.pallas_call(
        attention_kernel,
        grid=(blocks,),
        in_specs=[
            pl.BlockSpec(memory_space=pltpu.SMEM),
            pl.BlockSpec(memory_space=pltpu.SMEM),
            pl.BlockSpec((WINDOW, queries.shape[1]), lambda b: (b, 0)),
            pl.BlockSpec((2, WINDOW, width), lambda b: (0, jnp.maximum(b - 1, 0), 0)),
            pl.BlockSpec((2, WINDOW, width), lambda b: (0, b, 0)),
            pl.BlockSpec((2, WINDOW, width), lambda b: (0, 0, 0)),
        ],
        out_specs=pl.BlockSpec((WINDOW, queries.shape[1]), lambda b: (b, 0)),
        out_shape=jax.ShapeDtypeStruct(queries.shape, jnp.bfloat16),
        cost_estimate=pl.CostEstimate(flops=3 * 10**9, bytes_accessed=3 * 10**6, transcendentals=10**6),
        name="attention",
    )(first, sink_logits, queries, keys_values, keys_values, edge)


def dispatch_kernel(mine_ref, chosen_ref, rows_ref, gain_ref, out_ref, place_ref, normed_ref):
    f32 = jnp.float32
    bf16 = jnp.bfloat16
    tokens = rows_ref.shape[0]
    experts = 32
    capacity = 32
    values = rows_ref[...].astype(f32)
    mean = jnp.mean(values * values, axis=1, keepdims=True)
    normed = (values * lax.rsqrt(mean + 1e-06) * gain_ref[...]).astype(bf16)
    normed_ref[...] = normed * bf16(ROW_SCALE)
    which = lax.broadcasted_iota(jnp.int32, (experts, tokens), 0)
    first = (which == chosen_ref[0:1, :]).astype(f32)
    second = (which == chosen_ref[1:2, :]).astype(f32)
    before = (
        lax.broadcasted_iota(jnp.int32, (tokens, tokens), 0)
        < lax.broadcasted_iota(jnp.int32, (tokens, tokens), 1)
    ).astype(f32).astype(bf16)
    earlier = jnp.dot((first + second).astype(bf16), before, preferred_element_type=f32)
    places = []
    for k, hot in enumerate((first, second)):
        place = jnp.sum(hot * earlier, axis=0, keepdims=True).astype(jnp.int32)
        places.append(chosen_ref[k : k + 1, :] * capacity + place)
    slots = out_ref.shape[0]
    share = slots // experts
    slot = lax.broadcasted_iota(jnp.int32, (slots, tokens), 0)
    wanted = (slot // share) * capacity + mine_ref[0] * share + slot % share
    pick = ((places[0] == wanted) | (places[1] == wanted)).astype(f32).astype(bf16)
    out_ref[...] = jnp.dot(pick, normed_ref[...], preferred_element_type=f32).astype(bf16)
    for k in range(TOP):
        wide = jnp.broadcast_to(places[k].astype(f32), (LANES, tokens))
        place_ref[k] = wide.T.astype(jnp.int32)


def hidden_kernel(x_ref, gate_ref, up_ref, out_ref, hidden_ref):
    f32 = jnp.float32
    bf16 = jnp.bfloat16
    rows = x_ref.shape[0]
    step = 256
    back = f32(1.0 / ROW_SCALE)
    peak = jnp.zeros((8, LANES), f32)
    for i in range(rows // step):
        x = x_ref[i * step : (i + 1) * step, :]
        gate = jnp.dot(x, gate_ref[...], preferred_element_type=f32) * back
        up = jnp.dot(x, up_ref[...], preferred_element_type=f32) * back
        hidden = (gate / (1.0 + jnp.exp(-gate)) * up).astype(bf16)
        hidden_ref[i * step : (i + 1) * step, :] = hidden
        size = jnp.abs(hidden.astype(f32)).reshape(step // 8, 8, LANES)
        peak = jnp.maximum(peak, jnp.max(size, axis=0))
    top = jnp.max(jnp.max(peak, axis=1, keepdims=True), axis=0, keepdims=True)
    index = jnp.zeros((1, 1), f32)
    scale = jnp.full((1, 1), 2.0 ** (14 - EXP_LOW), f32)
    for i in range(1, EXP_COUNT):
        reached = top >= f32(2.0 ** (EXP_LOW + i))
        index = jnp.where(reached, f32(i), index)
        scale = jnp.where(reached, f32(2.0 ** (14 - EXP_LOW - i)), scale)
    for i in range(rows // step):
        part = hidden_ref[i * step : (i + 1) * step, :].astype(f32) * scale
        out_ref[i * step : (i + 1) * step, :] = part.astype(bf16)
    out_ref[rows:, :] = jnp.broadcast_to(index, (16, LANES)).astype(bf16)


def down_kernel(h_ref, w_ref, out_ref):
    f32 = jnp.float32
    bf16 = jnp.bfloat16
    blocks, extended, width = h_ref.shape
    rows = extended - 16
    weights = []
    for t in range(blocks):
        index = h_ref[t, rows : rows + 16, :].astype(f32)[0:1, :]
        scale = jnp.full((1, LANES), 2.0 ** (EXP_LOW - 14), f32)
        for i in range(1, EXP_COUNT):
            scale = jnp.where(index == f32(i), f32(2.0 ** (EXP_LOW - 14 + i)), scale)
        weights.append((w_ref[t * width : (t + 1) * width, :].astype(f32) * scale).astype(bf16))
    step = 256
    for i in range(rows // step):
        acc = jnp.zeros((step, w_ref.shape[1]), f32)
        for t in range(0, blocks, 2):
            left = h_ref[t, i * step : (i + 1) * step, :]
            right = h_ref[t + 1, i * step : (i + 1) * step, :]
            pair = jnp.concatenate([left, right], axis=1)
            weight = jnp.concatenate([weights[t], weights[t + 1]], axis=0)
            acc = acc + jnp.dot(pair, weight, preferred_element_type=f32)
        out_ref[i * step : (i + 1) * step, :] = acc.astype(bf16)


def combine_kernel(place_ref, weight_ref, rows_ref, out_ref):
    f32 = jnp.float32
    bf16 = jnp.bfloat16
    slots = rows_ref.shape[0]
    tokens = out_ref.shape[0]
    total = None
    for k in range(TOP):
        place = place_ref[k]
        hots = []
        for j in range(slots // LANES):
            slot = lax.broadcasted_iota(jnp.int32, (tokens, LANES), 1) + j * LANES
            hots.append((place == slot).astype(f32).astype(bf16))
        hot = jnp.concatenate(hots, axis=1)
        picked = jnp.dot(hot, rows_ref[...], preferred_element_type=f32)
        part = weight_ref[:, k : k + 1] * picked
        total = part if total is None else total + part
    out_ref[...] = total.astype(bf16)


def route_experts(
    moe_rows, norm_gain, group_choice, member_choice, route_weight, w_gate, w_up, w_down
):
    bf16 = jnp.bfloat16
    tokens, width = moe_rows.shape
    experts = 32
    capacity = 32
    tp = lax.axis_size("tp")
    share = capacity // tp
    slots = experts * share
    chosen = group_choice[None, :] * EPG + member_choice.T
    mine = lax.axis_index("tp").astype(jnp.int32).reshape(1)
    whole = pl.BlockSpec(memory_space=pltpu.VMEM)
    scalar = pl.BlockSpec(memory_space=pltpu.SMEM)
    outgoing, places = pl.pallas_call(
        dispatch_kernel,
        in_specs=[scalar, whole, whole, whole],
        out_specs=[whole, whole],
        out_shape=[
            jax.ShapeDtypeStruct((slots, width), bf16),
            jax.ShapeDtypeStruct((TOP, tokens, LANES), jnp.int32),
        ],
        scratch_shapes=[pltpu.VMEM((tokens, width), bf16)],
        name="dispatch",
    )(mine, chosen, moe_rows, norm_gain[None, :])
    incoming = lax.all_to_all(
        outgoing.reshape(experts, share * width // LANES, LANES), "ep", 0, 0, tiled=True
    )
    shared = incoming.reshape(slots, width).astype(jnp.float16)
    block_rows = lax.all_gather(shared, "tp", axis=0, tiled=True).astype(bf16)
    total = block_rows.shape[0]
    hidden = pl.pallas_call(
        hidden_kernel,
        in_specs=[whole, whole, whole],
        out_specs=whole,
        out_shape=jax.ShapeDtypeStruct((total + 16, w_gate.shape[2]), bf16),
        scratch_shapes=[pltpu.VMEM((total, w_gate.shape[2]), bf16)],
        name="hidden",
    )(block_rows, w_gate[0], w_up[0])
    spread = lax.all_gather(hidden.astype(jnp.float16), "tp", axis=0, tiled=False).astype(bf16)
    out_width = w_down.shape[2]
    produced = pl.pallas_call(
        down_kernel,
        in_specs=[whole, whole],
        out_specs=whole,
        out_shape=jax.ShapeDtypeStruct((total, out_width), bf16),
        name="down",
    )(spread, w_down[0])
    sources = lax.axis_size("ep")
    ordered = produced.reshape(tp, sources, share, out_width).transpose(1, 0, 2, 3)
    returned = lax.all_to_all(
        ordered.reshape(sources, capacity, out_width), "ep", 0, 0, tiled=True
    )
    return pl.pallas_call(
        combine_kernel,
        in_specs=[whole, whole, whole],
        out_specs=whole,
        out_shape=jax.ShapeDtypeStruct((tokens, out_width), bf16),
        name="combine",
    )(places, route_weight, returned.reshape(experts * capacity, out_width))


def shards(
    queries,
    keys_values,
    sink_logits,
    moe_rows,
    norm_gain,
    group_choice,
    member_choice,
    route_weight,
    w_gate,
    w_up,
    w_down,
):
    attended = attend_window(queries, keys_values, sink_logits)
    mixed = route_experts(
        moe_rows, norm_gain, group_choice, member_choice, route_weight, w_gate, w_up, w_down
    )
    return (attended, mixed)


def solution(mesh):
    in_specs = (
        P(("ep", "tp"), None),
        P(None, ("ep", "tp"), None),
        P(),
        P("ep", None),
        P(),
        P("ep"),
        P("ep", None),
        P("ep", None),
        P("ep", None, "tp"),
        P("ep", None, "tp"),
        P("ep", None, "tp"),
    )
    out_specs = (P(("ep", "tp"), None), P("ep", "tp"))
    return jax.shard_map(shards, mesh=mesh, in_specs=in_specs, out_specs=out_specs, check_vma=False)
```

time: 181 us -> 145 us (0.80)
  the two profiles are of different devices: /device:TPU:8 before, /device:TPU:64 now
where the time goes in v1:
time: 145 us; the launch traced here: 144 us
  blocking collectives  89.1 us (61%)
  Pallas kernels  24.3 us (17%)
  other arithmetic  8.64 us (6%)
  waiting for transfers between devices  8.08 us (6%)
  starting transfers between devices  7.09 us (5%)
  local copies, waits for them, and re-layouts  6.12 us (4%)
    all_gather x1, blocking collectives, route_experts(): block_rows = lax.all_gather(shared, 'tp', axis=0, tiled=True).astype(bf16)  32.3 us
    all_gather x1, blocking collectives, route_experts(): lax.all_gather(hidden.astype(jnp.float16), 'tp', axis=0, tiled=False)  32.3 us
    all_to_all x1, blocking collectives, route_experts(): lax.all_to_all(outgoing.reshape(experts, share * width // LANES, LANES),...  24.5 us
    pallas_call x1, Pallas kernels, attend_window(): pl.pallas_call(attention_kernel, grid=(blocks,), in_specs=[pl.BlockSpec(m...  9.24 us
    ppermute x1, waiting for transfers between devices, attend_window(): edge = lax.ppermute(edge_rows, ('ep', 'tp'), pairs)  8.08 us
    pallas_call x1, Pallas kernels, route_experts(): pl.pallas_call(hidden_kernel, in_specs=[whole, whole, whole], out_specs=w...  5.68 us
    all_to_all x1, starting transfers between devices, route_experts(): lax.all_to_all(ordered.reshape(sources, capacity, out_width), 'ep', 0, 0,...  5.17 us
    pallas_call x1, Pallas kernels, route_experts(): pl.pallas_call(down_kernel, in_specs=[whole, whole], out_specs=whole, out...  4.57 us
  transfers between devices with their start and end apart: 2, of which 1 were waited for; matrix products, arithmetic and copies ran while one was open for 1% of the time, Pallas kernels for 6%

profile of v1, /device:TPU:64, one launch (start us, length us, event | category | flops | bytes accessed | tf_op | source)
XLA Modules:
  0.0 144.0 jit_solution(2051525934639686013)
XLA Ops:
  0.6 0.7 broadcast_multiply_fusion
  1.3 1.3 add_bitcast_fusion.chosen_ref
  2.6 2.6 %dispatch.1 = (bf16[64,2048]{1,0:T(8,128)(2,1)}, s32[2,256,128]{2,1,0:T(8,128)}) custom-call(s32[1]{0:T(128)} %bitcast.1.mine_ref, s32[2,256]{1,0:T(2,128)} %add_bitcast_fusion.chosen_ref, bf16[256,2048]{1,0:T(8,128)(2,1)} %rows_ref.1, f32[1,2048]{1,0:T(1,128)} %bitcast.20), custom_call_target="tpu_custom_call" | custom-call | tf_op jit(solution)/shard_map/dispatch/pallas_call | solution.py:220
  5.2 1.1 reshape.31
  6.3 24.5 %all_to_all.10 = bf16[32,32,128]{2,1,0:T(8,128)(2,1)S(1)} all-to-all(bf16[32,32,128]{2,1,0:T(8,128)(2,1)S(1)} %reshape.31), channel_id=1, replica_groups=mesh['ep'=32,'tp'=16] {'ep'}, dimensions={0} | all-to-all | bytes 524288 | tf_op jit(solution)/shard_map/all_to_all | solution.py:231
  30.8 0.1 convert_element_type.16
  30.9 0.1 convert_element_type.17
  31.0 32.3 %all-gather.3 = f16[1024,2048]{1,0:T(8,128)(2,1)S(1)} all-gather(f16[64,2048]{1,0:T(8,128)(2,1)S(1)} %convert_element_type.17), channel_id=1, replica_groups=mesh['ep'=32,'tp'=16] {'tp'}, dimensions={0}, use_global_device_ids=true | all-gather | bytes 4456448 | tf_op jit(solution)/shard_map/all_gather | solution.py:235
  63.3 3.1 %convert_element_type.18.x_ref = bf16[1024,2048]{1,0:T(8,128)(2,1)} convert(f16[1024,2048]{1,0:T(8,128)(2,1)S(1)} %all-gather.3) | non-fusion elementwise | flops 2097152 | bytes 8388608 | tf_op jit(solution)/shard_map/convert_element_type | solution.py:235
  66.4 5.7 %hidden.1 = bf16[1040,128]{1,0:T(8,128)(2,1)} custom-call(bf16[1024,2048]{1,0:T(8,128)(2,1)} %convert_element_type.18.x_ref, bf16[2048,128]{1,0:T(8,128)(2,1)} %bitcast.17, bf16[2048,128]{1,0:T(8,128)(2,1)} %bitcast.18), custom_call_target="tpu_custom_call" | custom-call | tf_op jit(solution)/shard_map/hidden/pallas_call | solution.py:237
  72.1 1.0 convert_element_type.19
  73.1 32.3 %all-gather.4 = f16[16640,128]{1,0:T(8,128)(2,1)S(1)} all-gather(f16[1040,128]{1,0:T(8,128)(2,1)S(1)} %convert_element_type.19), channel_id=2, replica_groups=mesh['ep'=32,'tp'=16] {'tp'}, dimensions={0}, use_global_device_ids=true | all-gather | bytes 4526080 | tf_op jit(solution)/shard_map/all_gather | solution.py:245
  105.4 2.5 %convert_element_type.21 = bf16[16640,128]{1,0:T(8,128)(2,1)} convert(f16[16640,128]{1,0:T(8,128)(2,1)S(1)} %all-gather.4) | non-fusion elementwise | flops 2129920 | bytes 8519680 | tf_op jit(solution)/shard_map/convert_element_type | solution.py:245
  107.9 0.0 copy-start.1
  107.9 4.6 %down.1 = bf16[1024,128]{1,0:T(8,128)(2,1)} custom-call(bf16[16,1040,128]{2,1,0:T(8,128)(2,1)} %bitcast.14, bf16[2048,128]{1,0:T(8,128)(2,1)} %bitcast.19), custom_call_target="tpu_custom_call" | custom-call | tf_op jit(solution)/shard_map/down/pallas_call | solution.py:247
  112.5 1.8 %copy.13 = bf16[32,16,2,128]{3,2,1,0:T(2,128)(2,1)} copy(bf16[32,16,2,128]{3,2,0,1:T(2,128)(2,1)} %bitcast.15) | data formatting | bytes 524288 | tf_op jit(solution)/shard_map/transpose | solution.py:255
  114.3 5.2 %all-to-all-start.1 = ((bf16[32,32,128]{2,1,0:T(8,128)(2,1)}), bf16[32,32,128]{2,1,0:T(8,128)(2,1)S(1)}, u32[]{:S(2)}, u32[]{:S(2)}) async-start(bf16[32,32,128]{2,1,0:T(8,128)(2,1)} %bitcast.10), calls=%async_computation.1 | async-start | bytes 524288 | tf_op jit(solution)/shard_map/all_to_all | solution.py:256
  119.5 0.9 slice.3
  120.4 1.9 %collective-permute-start = (bf16[2,128,256]{2,1,0:T(8,128)(2,1)S(1)}, bf16[2,128,256]{2,1,0:T(8,128)(2,1)S(1)}, u32[]{:S(2)}, u32[]{:S(2)}) collective-permute-start(bf16[2,128,256]{2,1,0:T(8,128)(2,1)S(1)} %slice.3), channel_id=1, source_target_pairs={{0,1},{1,2},{2,3},{3,4},{4,5},{5,6},{6,7},{7,8},{8,9},{9,10},{10,1... | collective-permute-start | bytes 393224 | tf_op jit(solution)/shard_map/ppermute | solution.py:82
  122.3 0.0 copy-done.1
  122.4 0.8 copy.14.weight_ref
  123.2 8.1 %collective-permute-done.edge_ref = bf16[2,128,256]{2,1,0:T(8,128)(2,1)S(1)} collective-permute-done((bf16[2,128,256]{2,1,0:T(8,128)(2,1)S(1)}, bf16[2,128,256]{2,1,0:T(8,128)(2,1)S(1)}, u32[]{:S(2)}, u32[]{:S(2)}) %collective-permute-start) | collective-permute-done | bytes 131104 | tf_op jit(solution)/shard_map/ppermute | solution.py:82
  131.2 0.0 copy-start.2
  131.2 0.6 copy-done.2
  131.9 9.2 %attention.1 = bf16[384,1024]{1,0:T(8,128)(2,1)} custom-call(s32[1]{0:T(128)} %bitcast.first_ref, f32[16]{0:T(128)} %sink_ref.1, bf16[384,1024]{1,0:T(8,128)(2,1)} %q_ref.1, bf16[2,384,256]{2,1,0:T(8,128)(2,1)} %cur_ref.1, bf16[2,384,256]{2,1,0:T(8,128)(2,1)} %cur_ref.1, bf16[2,128,256]{2,1,0:T(8,128)(2,1)} %copy-done.2), custom_call_target="tpu_custom_call" | custom-call | flops 3000000000 | bytes 3000000 | tf_op jit(solution)/shard_map/attention/pallas_call | solution.py:84
  141.1 0.0 all-to-all-done.1
  141.1 0.0 copy-start
  141.1 0.7 copy-done
  141.8 2.2 %combine.1 = bf16[256,128]{1,0:T(8,128)(2,1)} custom-call(s32[2,256,128]{2,1,0:T(8,128)} %get-tuple-element.4.place_ref, f32[256,2]{1,0:T(8,128)} %copy.14.weight_ref, bf16[1024,128]{1,0:T(8,128)(2,1)} %bitcast.16), custom_call_target="tpu_custom_call" | custom-call | tf_op jit(solution)/shard_map/combine/pallas_call | solution.py:259
Async XLA Ops:
  107.9 14.4 %copy-start.1 = (f32[256,2]{0,1:T(2,128)S(1)}, f32[256,2]{0,1:T(2,128)}, u32[]{:S(2)}) copy-start(f32[256,2]{0,1:T(2,128)} %param.18) | copy-start | bytes 6148
  114.3 26.8 %all-to-all-start.1 = ((bf16[32,32,128]{2,1,0:T(8,128)(2,1)}), bf16[32,32,128]{2,1,0:T(8,128)(2,1)S(1)}, u32[]{:S(2)}, u32[]{:S(2)}) async-start(bf16[32,32,128]{2,1,0:T(8,128)(2,1)} %bitcast.10), calls=%async_computation.1 | async-start | bytes 524288 | tf_op jit(solution)/shard_map/all_to_all | solution.py:256
  120.4 10.8 %collective-permute-start = (bf16[2,128,256]{2,1,0:T(8,128)(2,1)S(1)}, bf16[2,128,256]{2,1,0:T(8,128)(2,1)S(1)}, u32[]{:S(2)}, u32[]{:S(2)}) collective-permute-start(bf16[2,128,256]{2,1,0:T(8,128)(2,1)S(1)} %slice.3), channel_id=1, source_target_pairs={{0,1},{1,2},{2,3},{3,4},{4,5},{5,6},{6,7},{7,8},{8,9},{9,10},{10,1... | collective-permute-start | bytes 393224 | tf_op jit(solution)/shard_map/ppermute | solution.py:82
  131.2 0.7 copy-start.2
  141.1 0.7 copy-start

commit v2 on v1

v2 whole, which is shorter than its diff:
```python
import jax
import jax.numpy as jnp
from jax import lax
from jax.experimental import pallas as pl
from jax.experimental.pallas import tpu as pltpu
from jax.sharding import PartitionSpec as P

QH = 16
KVH = 4
HD = 64
WINDOW = 128
EPG = 4
TOP = 2
LANES = 128
EXPERTS = 32
CAPACITY = 32
TP = 16
ROW_SCALE = 256.0
LEVELS = 11


def attention_kernel(first_ref, sink_ref, q_ref, prev_ref, cur_ref, edge_ref, out_ref):
    block = pl.program_id(0)
    f32 = jnp.float32
    bf16 = jnp.bfloat16
    row = lax.broadcasted_iota(jnp.int32, (WINDOW, WINDOW), 0)
    col = lax.broadcasted_iota(jnp.int32, (WINDOW, WINDOW), 1)
    causal = col <= row
    lane = lax.broadcasted_iota(jnp.int32, (WINDOW, LANES), 1)
    low = lane < HD
    at_start = block == 0
    hidden_prev = jnp.where(at_start, first_ref[0], 0)
    floor = jnp.where(hidden_prev == 1, f32(-1e30), f32(0.0))
    keep = jnp.where(hidden_prev == 1, f32(0.0), f32(1.0))
    zero = jnp.zeros((WINDOW, LANES), bf16)
    for c in range(KVH):
        lanes = pl.ds((c // 2) * LANES, LANES)
        mine = low if c % 2 == 0 else jnp.logical_not(low)
        parts = []
        for which in range(2):
            before = jnp.where(at_start, edge_ref[which, :, lanes], prev_ref[which, :, lanes])
            now = cur_ref[which, :, lanes]
            halves = []
            for value in (before, now):
                own = jnp.where(mine, value, zero)
                swapped = pltpu.roll(own.astype(f32), HD, 1).astype(bf16)
                halves.append((own, swapped) if c % 2 == 0 else (swapped, own))
            (a_prev, b_prev), (a_cur, b_cur) = halves
            parts.append(jnp.concatenate([a_prev, a_cur, b_prev, b_cur], axis=0))
        keys, values = parts
        keys = keys * bf16(HD ** (-0.5))
        for p in range(2):
            head = c * 4 + p * 2
            at = c * 256 + p * LANES
            q = q_ref[:, at : at + LANES]
            scores = lax.dot_general(q, keys, (((1,), (1,)), ((), ())), preferred_element_type=f32)
            pieces = []
            sums = []
            for side in range(2):
                base = side * 2 * WINDOW
                s_prev = scores[:, base : base + WINDOW] * keep + floor
                s_cur = scores[:, base + WINDOW : base + 2 * WINDOW]
                s = jnp.where(causal, s_cur, s_prev)
                sink = sink_ref[head + side]
                highest = jnp.maximum(jnp.max(s, axis=1, keepdims=True), sink)
                w = jnp.exp(s - highest)
                sums.append(jnp.sum(w, axis=1, keepdims=True) + jnp.exp(sink - highest))
                rounded = w.astype(bf16)
                pieces.append(jnp.where(causal, zero, rounded))
                pieces.append(jnp.where(causal, rounded, zero))
            weights = jnp.concatenate(pieces, axis=1)
            summed = jnp.dot(weights, values, preferred_element_type=f32)
            total = jnp.where(low, sums[0], sums[1])
            out_ref[:, at : at + LANES] = (summed / total).astype(bf16)


def edge_of(keys_values):
    length = keys_values.shape[1]
    peers = lax.axis_size(("ep", "tp"))
    pairs = [(i, i + 1) for i in range(peers - 1)]
    return lax.ppermute(keys_values[:, length - WINDOW :, :], ("ep", "tp"), pairs)


def attend_window(queries, keys_values, sink_logits, edge):
    blocks = queries.shape[0] // WINDOW
    width = keys_values.shape[2]
    first = (lax.axis_index(("ep", "tp")) == 0).astype(jnp.int32).reshape(1)
    return pl.pallas_call(
        attention_kernel,
        grid=(blocks,),
        in_specs=[
            pl.BlockSpec(memory_space=pltpu.SMEM),
            pl.BlockSpec(memory_space=pltpu.SMEM),
            pl.BlockSpec((WINDOW, queries.shape[1]), lambda b: (b, 0)),
            pl.BlockSpec((2, WINDOW, width), lambda b: (0, jnp.maximum(b - 1, 0), 0)),
            pl.BlockSpec((2, WINDOW, width), lambda b: (0, b, 0)),
            pl.BlockSpec((2, WINDOW, width), lambda b: (0, 0, 0)),
        ],
        out_specs=pl.BlockSpec((WINDOW, queries.shape[1]), lambda b: (b, 0)),
        out_shape=jax.ShapeDtypeStruct(queries.shape, jnp.bfloat16),
        cost_estimate=pl.CostEstimate(flops=3 * 10**9, bytes_accessed=3 * 10**6, transcendentals=10**6),
        name="attention",
    )(first, sink_logits, queries, keys_values, keys_values, edge)


def dispatch_kernel(mine_ref, group_ref, member_ref, rows_ref, gain_ref, out_ref, place_ref, normed_ref):
    f32 = jnp.float32
    bf16 = jnp.bfloat16
    tokens = rows_ref.shape[0]
    values = rows_ref[...].astype(f32)
    mean = jnp.mean(values * values, axis=1, keepdims=True)
    normed = (values * lax.rsqrt(mean + 1e-06) * gain_ref[...]).astype(bf16)
    normed_ref[...] = normed * bf16(ROW_SCALE)
    chosen = group_ref[...] * EPG + member_ref[...]
    which = lax.broadcasted_iota(jnp.int32, (EXPERTS, tokens), 0)
    first = (which == chosen[0:1, :]).astype(f32)
    second = (which == chosen[1:2, :]).astype(f32)
    before = (
        lax.broadcasted_iota(jnp.int32, (tokens, tokens), 0)
        < lax.broadcasted_iota(jnp.int32, (tokens, tokens), 1)
    ).astype(f32).astype(bf16)
    earlier = jnp.dot((first + second).astype(bf16), before, preferred_element_type=f32)
    places = []
    for k, hot in enumerate((first, second)):
        place = jnp.sum(hot * earlier, axis=0, keepdims=True).astype(jnp.int32)
        places.append(chosen[k : k + 1, :] * CAPACITY + place)
        place_ref[k : k + 1, :] = places[k]
    slots = out_ref.shape[0]
    share = slots // EXPERTS
    slot = lax.broadcasted_iota(jnp.int32, (slots, tokens), 0)
    wanted = (slot // share) * CAPACITY + mine_ref[0] * share + slot % share
    pick = ((places[0] == wanted) | (places[1] == wanted)).astype(f32).astype(bf16)
    out_ref[...] = jnp.dot(pick, normed_ref[...], preferred_element_type=f32).astype(bf16)


def prepare_kernel(place_ref, weight_ref, hot_ref, column_ref):
    f32 = jnp.float32
    bf16 = jnp.bfloat16
    tokens = place_ref.shape[1]
    slots = hot_ref.shape[2]
    for k in range(TOP):
        wide = jnp.broadcast_to(place_ref[k : k + 1, :].astype(f32), (LANES, tokens))
        place = wide.T.astype(jnp.int32)
        for j in range(slots // LANES):
            slot = lax.broadcasted_iota(jnp.int32, (tokens, LANES), 1) + j * LANES
            hot_ref[k, :, j * LANES : (j + 1) * LANES] = (place == slot).astype(f32).astype(bf16)
        column_ref[k] = jnp.broadcast_to(weight_ref[k : k + 1, :], (LANES, tokens)).T


def hidden_kernel(y_ref, out_ref, plain_ref, ordered_ref):
    f32 = jnp.float32
    bf16 = jnp.bfloat16
    rows, width = plain_ref.shape
    share = CAPACITY // TP
    sources = rows // CAPACITY
    back = f32(1.0 / ROW_SCALE)
    peak = jnp.zeros((8, width), f32)
    step = share * sources
    for i in range(TP):
        gate = y_ref[i * step : (i + 1) * step, :width] * back
        up = y_ref[i * step : (i + 1) * step, width:] * back
        hidden = (gate / (1.0 + jnp.exp(-gate)) * up).astype(bf16).astype(f32)
        plain_ref[i * step : (i + 1) * step, :] = hidden
        peak = jnp.maximum(peak, jnp.max(jnp.abs(hidden).reshape(step // 8, 8, width), axis=0))
    top = jnp.max(jnp.max(peak, axis=1, keepdims=True), axis=0, keepdims=True)
    index = jnp.zeros((1, 1), f32)
    scale = jnp.full((1, 1), 2.0**71, f32)
    for i in range(1, LEVELS):
        reached = top >= f32(2.0 ** (8 * i - 64))
        index = jnp.where(reached, f32(i), index)
        scale = jnp.where(reached, f32(2.0 ** (71 - 8 * i)), scale)
    for i in range(TP):
        for j in range(share):
            part = plain_ref[pl.ds(i * step + j, sources, stride=share), :]
            ordered_ref[pl.ds(i * share + j, sources, stride=CAPACITY), :] = part
    out_ref[:rows, :] = (ordered_ref[...] * scale).astype(bf16)
    out_ref[rows:, :] = jnp.broadcast_to(index, (16, width)).astype(bf16)


def combine_kernel(hot_ref, column_ref, rows_ref, out_ref):
    total = None
    for k in range(TOP):
        picked = jnp.dot(hot_ref[k], rows_ref[...], preferred_element_type=jnp.float32)
        part = column_ref[k] * picked
        total = part if total is None else total + part
    out_ref[...] = total.astype(jnp.bfloat16)


def near(value):
    return pltpu.with_memory_space_constraint(value, pltpu.VMEM)


def route_experts(
    moe_rows, norm_gain, group_choice, member_choice, route_weight, w_gate, w_up, w_down, edge
):
    bf16 = jnp.bfloat16
    tokens, width = moe_rows.shape
    share = CAPACITY // TP
    slots = EXPERTS * share
    mine = lax.axis_index("tp").astype(jnp.int32).reshape(1)
    whole = pl.BlockSpec(memory_space=pltpu.VMEM)
    scalar = pl.BlockSpec(memory_space=pltpu.SMEM)
    outgoing, places = pl.pallas_call(
        dispatch_kernel,
        in_specs=[scalar, whole, whole, whole, whole],
        out_specs=[whole, whole],
        out_shape=[
            pltpu.VMEM((slots, width), bf16),
            pltpu.VMEM((TOP, tokens), jnp.int32),
        ],
        scratch_shapes=[pltpu.VMEM((tokens, width), bf16)],
        name="dispatch",
    )(mine, group_choice[None, :], member_choice.T, moe_rows, norm_gain[None, :])
    incoming = lax.all_to_all(
        outgoing.reshape(EXPERTS, share * width // LANES, LANES), "ep", 0, 0, tiled=True
    )
    hots, columns = pl.pallas_call(
        prepare_kernel,
        in_specs=[whole, whole],
        out_specs=[whole, whole],
        out_shape=[
            pltpu.VMEM((TOP, tokens, EXPERTS * CAPACITY), bf16),
            pltpu.VMEM((TOP, tokens, LANES), jnp.float32),
        ],
        name="prepare",
    )(places, route_weight.T)
    both = jnp.concatenate([w_gate[0], w_up[0]], axis=1)
    incoming, edge, hots, columns, both = lax.optimization_barrier(
        (incoming, edge, hots, columns, both)
    )
    shared = incoming.reshape(slots, width).astype(jnp.float16)
    block_rows = lax.all_gather(shared, "tp", axis=0, tiled=True).astype(bf16)
    total = block_rows.shape[0]
    y = jnp.dot(block_rows, both, preferred_element_type=jnp.float32)
    units = w_gate.shape[2]
    hidden = pl.pallas_call(
        hidden_kernel,
        in_specs=[whole],
        out_specs=whole,
        out_shape=pltpu.VMEM((total + 16, units), bf16),
        scratch_shapes=[pltpu.VMEM((total, units), jnp.float32)] * 2,
        name="hidden",
    )(near(y))
    spread = lax.all_gather(hidden.astype(jnp.float16), "tp", axis=0, tiled=False)
    index = spread[:, total, 0].astype(jnp.float32)
    factor = jnp.full(index.shape, 2.0**-71, jnp.float32)
    for i in range(1, LEVELS):
        factor = jnp.where(index == i, 2.0 ** (8 * i - 71), factor)
    out_width = w_down.shape[2]
    weight = w_down[0].reshape(TP, units, out_width).astype(jnp.float32) * factor[:, None, None]
    produced = jnp.einsum(
        "trk,tko->ro",
        spread.astype(bf16),
        weight.astype(bf16),
        preferred_element_type=jnp.float32,
    ).astype(bf16)[:total]
    returned = lax.all_to_all(
        produced.reshape(total // CAPACITY, CAPACITY, out_width), "ep", 0, 0, tiled=True
    )
    mixed = pl.pallas_call(
        combine_kernel,
        in_specs=[whole, whole, whole],
        out_specs=whole,
        out_shape=jax.ShapeDtypeStruct((tokens, out_width), bf16),
        name="combine",
    )(near(hots), near(columns), near(returned.reshape(EXPERTS * CAPACITY, out_width)))
    return mixed, edge, produced


def shards(
    queries,
    keys_values,
    sink_logits,
    moe_rows,
    norm_gain,
    group_choice,
    member_choice,
    route_weight,
    w_gate,
    w_up,
    w_down,
):
    edge = edge_of(keys_values)
    mixed, edge, produced = route_experts(
        moe_rows,
        norm_gain,
        group_choice,
        member_choice,
        route_weight,
        w_gate,
        w_up,
        w_down,
        edge,
    )
    sink_logits, produced = lax.optimization_barrier((sink_logits, produced))
    attended = attend_window(queries, keys_values, sink_logits, edge)
    return (attended, mixed)


def solution(mesh):
    in_specs = (
        P(("ep", "tp"), None),
        P(None, ("ep", "tp"), None),
        P(),
        P("ep", None),
        P(),
        P("ep"),
        P("ep", None),
        P("ep", None),
        P("ep", None, "tp"),
        P("ep", None, "tp"),
        P("ep", None, "tp"),
    )
    out_specs = (P(("ep", "tp"), None), P("ep", "tp"))
    return jax.shard_map(shards, mesh=mesh, in_specs=in_specs, out_specs=out_specs, check_vma=False)
```

time: 145 us -> 121 us (0.83)
  the two profiles are of different devices: /device:TPU:64 before, /device:TPU:8 now
where the time goes in v2:
time: 121 us; the launch traced here: 120 us
  blocking collectives  64.4 us (53%)
  starting transfers between devices  22.5 us (19%)
  Pallas kernels  13.9 us (11%)
  waiting for transfers between devices  10.9 us (9%)
  local copies, waits for them, and re-layouts  2.62 us (2%)
  matrix products  2.61 us (2%)
  other arithmetic  2.6 us (2%)
    all_gather x1, blocking collectives, route_experts(): lax.all_gather(hidden.astype(jnp.float16), 'tp', axis=0, tiled=False)  34.4 us
    all_gather x1, blocking collectives, route_experts(): block_rows = lax.all_gather(shared, 'tp', axis=0, tiled=True).astype(bf16)  30 us
    all_to_all x1, starting transfers between devices, route_experts(): lax.all_to_all(outgoing.reshape(EXPERTS, share * width // LANES, LANES),...  13.2 us
    pallas_call x1, Pallas kernels, attend_window(): pl.pallas_call(attention_kernel, grid=(blocks,), in_specs=[pl.BlockSpec(m...  9.28 us
    all_to_all x1, starting transfers between devices, route_experts(): lax.all_to_all(produced.reshape(total // CAPACITY, CAPACITY, out_width),...  7.42 us
    all_to_all x1, waiting for transfers between devices, route_experts(): lax.all_to_all(outgoing.reshape(EXPERTS, share * width // LANES, LANES),...  5.59 us
    all_to_all x1, waiting for transfers between devices, route_experts(): lax.all_to_all(produced.reshape(total // CAPACITY, CAPACITY, out_width),...  4.28 us
  transfers between devices with their start and end apart: 3, of which 3 were waited for; matrix products, arithmetic and copies ran while one was open for 3% of the time, Pallas kernels for 9%

profile of v2, /device:TPU:8, one launch (start us, length us, event | category | flops | bytes accessed | tf_op | source)
XLA Modules:
  0.0 120.3 jit_solution(15406213838430802652)
XLA Ops:
  0.6 1.9 %dispatch.1 = (bf16[64,2048]{1,0:T(8,128)(2,1)S(1)}, s32[2,256]{1,0:T(2,128)S(1)}) custom-call(s32[1]{0:T(128)} %bitcast.1.mine_ref, s32[1,256]{1,0:T(1,128)} %bitcast.24, s32[2,256]{1,0:T(2,128)} %bitcast.22, bf16[256,2048]{1,0:T(8,128)(2,1)} %rows_ref.1, f32[1,2048]{1,0:T(1,128)} %bitcast.21), custom_call_target="tpu_custom_call" | custom-call | tf_op jit(solution)/shard_map/dispatch/pallas_call | solution.py:203
  2.6 0.0 copy-start
  2.6 0.8 reshape.28
  3.4 13.2 %all-to-all-start = ((bf16[32,32,128]{2,1,0:T(8,128)(2,1)}), bf16[32,32,128]{2,1,0:T(8,128)(2,1)S(1)}, u32[]{:S(2)}, u32[]{:S(2)}) async-start(bf16[32,32,128]{2,1,0:T(8,128)(2,1)} %reshape.28), calls=%async_computation | async-start | bytes 524288 | tf_op jit(solution)/shard_map/all_to_all | solution.py:214
  16.6 0.9 slice.9
  17.5 1.9 %collective-permute-start = (bf16[2,128,256]{2,1,0:T(8,128)(2,1)S(1)}, bf16[2,128,256]{2,1,0:T(8,128)(2,1)S(1)}, u32[]{:S(2)}, u32[]{:S(2)}) collective-permute-start(bf16[2,128,256]{2,1,0:T(8,128)(2,1)S(1)} %slice.9), channel_id=1, source_target_pairs={{0,1},{1,2},{2,3},{3,4},{4,5},{5,6},{6,7},{7,8},{8,9},{9,10},{10,1... | collective-permute-start | bytes 393224 | tf_op jit(solution)/shard_map/ppermute | solution.py:81
  19.4 0.0 copy-done
  19.4 1.0 prepare.1
  20.4 2.3 %pad_maximum_fusion = bf16[2048,256]{1,0:T(8,128)(2,1)} fusion(bf16[2048,128]{1,0:T(8,128)(2,1)} %bitcast.19, bf16[2048,128]{1,0:T(8,128)(2,1)} %bitcast.20), kind=kLoop, calls=%fused_computation.5 | loop fusion | flops 2097152 | bytes 2097152 | tf_op jit(solution)/shard_map/concatenate | solution.py:227
  22.7 1.1 collective-permute-done.edge_ref
  23.8 0.0 copy-start.3
  23.8 5.6 %all-to-all-done = bf16[32,32,128]{2,1,0:T(8,128)(2,1)S(1)} async-done(((bf16[32,32,128]{2,1,0:T(8,128)(2,1)}), bf16[32,32,128]{2,1,0:T(8,128)(2,1)S(1)}, u32[]{:S(2)}, u32[]{:S(2)}) %all-to-all-start) | async-done | bytes 262176 | tf_op jit(solution)/shard_map/all_to_all | solution.py:214
  29.4 0.1 convert_element_type.32
  29.4 0.1 convert_element_type.33
  29.6 0.0 copy-start.1
  29.6 30.0 %all-gather.3 = f16[1024,2048]{1,0:T(8,128)(2,1)S(1)} all-gather(f16[64,2048]{1,0:T(8,128)(2,1)S(1)} %convert_element_type.33), channel_id=1, replica_groups=mesh['ep'=32,'tp'=16] {'tp'}, dimensions={0}, use_global_device_ids=true | all-gather | bytes 4456448 | tf_op jit(solution)/shard_map/all_gather | solution.py:232
  59.6 0.0 copy-done.1
  59.6 1.3 %fusion.2.y_ref = f32[1024,256]{1,0:T(8,128)S(1)} fusion(bf16[2048,256]{1,0:T(8,128)(2,1)S(1)} %copy-done.1, f16[1024,2048]{1,0:T(8,128)(2,1)S(1)} %all-gather.3), kind=kOutput, calls=%fused_computation.2 | convolution fusion | flops 1075838976 | bytes 6291456 | tf_op jit(solution)/shard_map/dot_general | solution.py:234
  60.8 0.0 copy-done.3
  60.8 0.6 hidden.1
  61.5 0.0 copy-start.2
  61.5 0.1 convert_element_type.35
  61.6 34.4 %all-gather.4 = f16[16640,128]{1,0:T(8,128)(2,1)S(1)} all-gather(f16[1040,128]{1,0:T(8,128)(2,1)S(1)} %convert_element_type.35), channel_id=2, replica_groups=mesh['ep'=32,'tp'=16] {'tp'}, dimensions={0}, use_global_device_ids=true | all-gather | bytes 4526080 | tf_op jit(solution)/shard_map/all_gather | solution.py:244
  96.0 0.2 fusion.10
  96.2 0.0 copy-done.2
  96.2 1.4 %fusion.4 = bf16[1040,128]{1,0:T(8,128)(2,1)S(1)} fusion(f16[16,1040,128]{2,1,0:T(8,128)(2,1)S(1)} %bitcast.18, bf16[16,128,128]{2,1,0:T(8,128)(2,1)S(1)} %bitcast.25, f32[16]{0:T(128)S(1)} %fusion.10), kind=kOutput, calls=%fused_computation.4 | convolution fusion | flops 548175872 | bytes 5050432 | tf_op jit(solution)/shard_map/trk,tko->ro/dot_general | solution.py:251
  97.6 0.7 slice.20
  98.3 7.4 %all-to-all-start.1 = ((bf16[32,32,128]{2,1,0:T(8,128)(2,1)}), bf16[32,32,128]{2,1,0:T(8,128)(2,1)S(1)}, u32[]{:S(2)}, u32[]{:S(2)}) async-start(bf16[32,32,128]{2,1,0:T(8,128)(2,1)} %bitcast.11), calls=%async_computation.1 | async-start | bytes 524288 | tf_op jit(solution)/shard_map/all_to_all | solution.py:257
  105.7 9.3 %attention.1 = bf16[384,1024]{1,0:T(8,128)(2,1)} custom-call(s32[1]{0:T(128)} %bitcast.first_ref, f32[16]{0:T(128)} %sink_ref, bf16[384,1024]{1,0:T(8,128)(2,1)} %q_ref.1, bf16[2,384,256]{2,1,0:T(8,128)(2,1)} %cur_ref.1, bf16[2,384,256]{2,1,0:T(8,128)(2,1)} %cur_ref.1, bf16[2,128,256]{2,1,0:T(8,128)(2,1)} %copy-done.3), custom_call_target="tpu_custom_call" | custom-call | flops 3000000000 | bytes 3000000 | tf_op jit(solution)/shard_map/attention/pallas_call | solution.py:88
  115.0 4.3 %all-to-all-done.1 = bf16[32,32,128]{2,1,0:T(8,128)(2,1)S(1)} async-done(((bf16[32,32,128]{2,1,0:T(8,128)(2,1)}), bf16[32,32,128]{2,1,0:T(8,128)(2,1)S(1)}, u32[]{:S(2)}, u32[]{:S(2)}) %all-to-all-start.1) | async-done | bytes 262176 | tf_op jit(solution)/shard_map/all_to_all | solution.py:257
  119.3 1.1 combine.1
Async XLA Ops:
  2.6 16.9 %copy-start = (s32[2,256]{1,0:T(2,128)}, s32[2,256]{1,0:T(2,128)S(1)}, u32[]{:S(2)}) copy-start(s32[2,256]{1,0:T(2,128)S(1)} %get-tuple-element.13.place_ref) | copy-start | bytes 6148
  3.4 26.0 %all-to-all-start = ((bf16[32,32,128]{2,1,0:T(8,128)(2,1)}), bf16[32,32,128]{2,1,0:T(8,128)(2,1)S(1)}, u32[]{:S(2)}, u32[]{:S(2)}) async-start(bf16[32,32,128]{2,1,0:T(8,128)(2,1)} %reshape.28), calls=%async_computation | async-start | bytes 524288 | tf_op jit(solution)/shard_map/all_to_all | solution.py:214
  17.5 6.3 %collective-permute-start = (bf16[2,128,256]{2,1,0:T(8,128)(2,1)S(1)}, bf16[2,128,256]{2,1,0:T(8,128)(2,1)S(1)}, u32[]{:S(2)}, u32[]{:S(2)}) collective-permute-start(bf16[2,128,256]{2,1,0:T(8,128)(2,1)S(1)} %slice.9), channel_id=1, source_target_pairs={{0,1},{1,2},{2,3},{3,4},{4,5},{5,6},{6,7},{7,8},{8,9},{9,10},{10,1... | collective-permute-start | bytes 393224 | tf_op jit(solution)/shard_map/ppermute | solution.py:81
  23.8 37.1 %copy-start.3 = (bf16[2,128,256]{2,1,0:T(8,128)(2,1)}, bf16[2,128,256]{2,1,0:T(8,128)(2,1)S(1)}, u32[]{:S(2)}) copy-start(bf16[2,128,256]{2,1,0:T(8,128)(2,1)S(1)} %collective-permute-done.edge_ref) | copy-start | bytes 393220
  29.6 30.0 %copy-start.1 = (bf16[2048,256]{1,0:T(8,128)(2,1)S(1)}, bf16[2048,256]{1,0:T(8,128)(2,1)}, u32[]{:S(2)}) copy-start(bf16[2048,256]{1,0:T(8,128)(2,1)} %pad_maximum_fusion) | copy-start | bytes 3145732
  61.5 34.7 %copy-start.2 = (bf16[1,2048,128]{2,1,0:T(8,128)(2,1)S(1)}, bf16[1,2048,128]{2,1,0:T(8,128)(2,1)}, u32[]{:S(2)}) copy-start(bf16[1,2048,128]{2,1,0:T(8,128)(2,1)} %param.21) | copy-start | bytes 1572868
  98.3 21.0 %all-to-all-start.1 = ((bf16[32,32,128]{2,1,0:T(8,128)(2,1)}), bf16[32,32,128]{2,1,0:T(8,128)(2,1)S(1)}, u32[]{:S(2)}, u32[]{:S(2)}) async-start(bf16[32,32,128]{2,1,0:T(8,128)(2,1)} %bitcast.11), calls=%async_computation.1 | async-start | bytes 524288 | tf_op jit(solution)/shard_map/all_to_all | solution.py:257

commit v3 on v2

--- a/solution.py
+++ b/solution.py
@@ -19,59 +19,80 @@
 LEVELS = 11
 
 
-def attention_kernel(first_ref, sink_ref, q_ref, prev_ref, cur_ref, edge_ref, out_ref):
-    block = pl.program_id(0)
+def near(value):
+    return pltpu.with_memory_space_constraint(value, pltpu.VMEM)
+
+
+def attention_kernel(first_ref, sink_ref, q_ref, kv_ref, edge_ref, out_ref, band_ref):
     f32 = jnp.float32
     bf16 = jnp.bfloat16
+    blocks = q_ref.shape[0] // WINDOW
     row = lax.broadcasted_iota(jnp.int32, (WINDOW, WINDOW), 0)
     col = lax.broadcasted_iota(jnp.int32, (WINDOW, WINDOW), 1)
     causal = col <= row
-    lane = lax.broadcasted_iota(jnp.int32, (WINDOW, LANES), 1)
-    low = lane < HD
-    at_start = block == 0
-    hidden_prev = jnp.where(at_start, first_ref[0], 0)
-    floor = jnp.where(hidden_prev == 1, f32(-1e30), f32(0.0))
-    keep = jnp.where(hidden_prev == 1, f32(0.0), f32(1.0))
+    low = lax.broadcasted_iota(jnp.int32, (WINDOW, LANES), 1) < HD
     zero = jnp.zeros((WINDOW, LANES), bf16)
-    for c in range(KVH):
-        lanes = pl.ds((c // 2) * LANES, LANES)
-        mine = low if c % 2 == 0 else jnp.logical_not(low)
-        parts = []
-        for which in range(2):
-            before = jnp.where(at_start, edge_ref[which, :, lanes], prev_ref[which, :, lanes])
-            now = cur_ref[which, :, lanes]
-            halves = []
-            for value in (before, now):
-                own = jnp.where(mine, value, zero)
-                swapped = pltpu.roll(own.astype(f32), HD, 1).astype(bf16)
-                halves.append((own, swapped) if c % 2 == 0 else (swapped, own))
-            (a_prev, b_prev), (a_cur, b_cur) = halves
-            parts.append(jnp.concatenate([a_prev, a_cur, b_prev, b_cur], axis=0))
-        keys, values = parts
-        keys = keys * bf16(HD ** (-0.5))
-        for p in range(2):
-            head = c * 4 + p * 2
-            at = c * 256 + p * LANES
-            q = q_ref[:, at : at + LANES]
+    for which in range(2):
+        for part in range(blocks + 1):
+            for h in range(KVH // 2):
+                lanes = slice(h * LANES, (h + 1) * LANES)
+                if part == 0:
+                    value = edge_ref[which, :, lanes]
+                else:
+                    value = kv_ref[which, (part - 1) * WINDOW : part * WINDOW, lanes]
+                if which == 0:
+                    value = value * bf16(HD ** (-0.5))
+                turned = pltpu.roll(value.astype(f32), HD, 1).astype(bf16)
+                at = slice(part * WINDOW, (part + 1) * WINDOW)
+                band_ref[which, 2 * h, 0, at, :] = jnp.where(low, value, zero)
+                band_ref[which, 2 * h, 1, at, :] = jnp.where(low, zero, turned)
+                band_ref[which, 2 * h + 1, 0, at, :] = jnp.where(low, turned, zero)
+                band_ref[which, 2 * h + 1, 1, at, :] = jnp.where(low, zero, value)
+
+    absent = jnp.where(first_ref[0] == 1, f32(-1e30), f32(0.0))
+    bias = jnp.where(causal, f32(0.0), absent)
+    for block in range(blocks):
+        start = block * WINDOW
+        band = pl.ds(start, 2 * WINDOW)
+        for c in range(KVH):
+            keys = jnp.concatenate([band_ref[0, c, 0, band, :], band_ref[0, c, 1, band, :]], axis=0)
+            values = jnp.concatenate([band_ref[1, c, 0, band, :], band_ref[1, c, 1, band, :]], axis=0)
+            q = jnp.concatenate(
+                [q_ref[pl.ds(start, WINDOW), c * 256 + p * LANES : c * 256 + (p + 1) * LANES] for p in range(2)],
+                axis=0,
+            )
             scores = lax.dot_general(q, keys, (((1,), (1,)), ((), ())), preferred_element_type=f32)
-            pieces = []
-            sums = []
-            for side in range(2):
-                base = side * 2 * WINDOW
-                s_prev = scores[:, base : base + WINDOW] * keep + floor
-                s_cur = scores[:, base + WINDOW : base + 2 * WINDOW]
-                s = jnp.where(causal, s_cur, s_prev)
-                sink = sink_ref[head + side]
-                highest = jnp.maximum(jnp.max(s, axis=1, keepdims=True), sink)
-                w = jnp.exp(s - highest)
-                sums.append(jnp.sum(w, axis=1, keepdims=True) + jnp.exp(sink - highest))
-                rounded = w.astype(bf16)
-                pieces.append(jnp.where(causal, zero, rounded))
-                pieces.append(jnp.where(causal, rounded, zero))
-            weights = jnp.concatenate(pieces, axis=1)
-            summed = jnp.dot(weights, values, preferred_element_type=f32)
-            total = jnp.where(low, sums[0], sums[1])
-            out_ref[:, at : at + LANES] = (summed / total).astype(bf16)
+            lines = []
+            totals = []
+            for p in range(2):
+                head = c * 4 + p * 2
+                pieces = []
+                sums = []
+                tops = []
+                for side in range(2):
+                    base = side * 2 * WINDOW
+                    s_prev = scores[p * WINDOW : (p + 1) * WINDOW, base : base + WINDOW]
+                    s_cur = scores[p * WINDOW : (p + 1) * WINDOW, base + WINDOW : base + 2 * WINDOW]
+                    s = jnp.where(causal, s_cur, s_prev)
+                    if block == 0:
+                        s = s + bias
+                    highest = jnp.maximum(jnp.max(s, axis=1, keepdims=True), sink_ref[head + side])
+                    w = jnp.exp(s - highest)
+                    sums.append(jnp.sum(w, axis=1, keepdims=True))
+                    tops.append(highest)
+                    rounded = w.astype(bf16)
+                    pieces.append(jnp.where(causal, zero, rounded))
+                    pieces.append(jnp.where(causal, rounded, zero))
+                lines.append(jnp.concatenate(pieces, axis=1))
+                sink = jnp.where(low, sink_ref[head], sink_ref[head + 1])
+                rest = jnp.exp(sink - jnp.where(low, tops[0], tops[1]))
+                totals.append(jnp.where(low, sums[0], sums[1]) + rest)
+            summed = jnp.dot(jnp.concatenate(lines, axis=0), values, preferred_element_type=f32)
+            for p in range(2):
+                at = c * 256 + p * LANES
+                out_ref[pl.ds(start, WINDOW), at : at + LANES] = (
+                    summed[p * WINDOW : (p + 1) * WINDOW] / totals[p]
+                ).astype(bf16)
 
 
 def edge_of(keys_values):
@@ -82,31 +103,26 @@
 
 
 def attend_window(queries, keys_values, sink_logits, edge):
-    blocks = queries.shape[0] // WINDOW
-    width = keys_values.shape[2]
     first = (lax.axis_index(("ep", "tp")) == 0).astype(jnp.int32).reshape(1)
+    whole = pl.BlockSpec(memory_space=pltpu.VMEM)
+    scalar = pl.BlockSpec(memory_space=pltpu.SMEM)
+    rows = keys_values.shape[1] + WINDOW
     return pl.pallas_call(
         attention_kernel,
-        grid=(blocks,),
-        in_specs=[
-            pl.BlockSpec(memory_space=pltpu.SMEM),
-            pl.BlockSpec(memory_space=pltpu.SMEM),
-            pl.BlockSpec((WINDOW, queries.shape[1]), lambda b: (b, 0)),
-            pl.BlockSpec((2, WINDOW, width), lambda b: (0, jnp.maximum(b - 1, 0), 0)),
-            pl.BlockSpec((2, WINDOW, width), lambda b: (0, b, 0)),
-            pl.BlockSpec((2, WINDOW, width), lambda b: (0, 0, 0)),
-        ],
-        out_specs=pl.BlockSpec((WINDOW, queries.shape[1]), lambda b: (b, 0)),
+        in_specs=[scalar, scalar, whole, whole, whole],
+        out_specs=whole,
         out_shape=jax.ShapeDtypeStruct(queries.shape, jnp.bfloat16),
+        scratch_shapes=[pltpu.VMEM((2, KVH, 2, rows, LANES), jnp.bfloat16)],
         cost_estimate=pl.CostEstimate(flops=3 * 10**9, bytes_accessed=3 * 10**6, transcendentals=10**6),
         name="attention",
-    )(first, sink_logits, queries, keys_values, keys_values, edge)
-
-
-def dispatch_kernel(mine_ref, group_ref, member_ref, rows_ref, gain_ref, out_ref, place_ref, normed_ref):
+    )(first, sink_logits, near(queries), near(keys_values), near(edge))
+
+
+def dispatch_kernel(mine_ref, group_ref, member_ref, rows_ref, gain_ref, out_ref, place_ref, normed_ref, line_ref):
     f32 = jnp.float32
     bf16 = jnp.bfloat16
-    tokens = rows_ref.shape[0]
+    tokens, width = rows_ref.shape
+    pieces = width // LANES
     values = rows_ref[...].astype(f32)
     mean = jnp.mean(values * values, axis=1, keepdims=True)
     normed = (values * lax.rsqrt(mean + 1e-06) * gain_ref[...]).astype(bf16)
@@ -125,12 +141,15 @@
         place = jnp.sum(hot * earlier, axis=0, keepdims=True).astype(jnp.int32)
         places.append(chosen[k : k + 1, :] * CAPACITY + place)
         place_ref[k : k + 1, :] = places[k]
-    slots = out_ref.shape[0]
-    share = slots // EXPERTS
+    share = CAPACITY // TP
+    slots = EXPERTS * share
     slot = lax.broadcasted_iota(jnp.int32, (slots, tokens), 0)
     wanted = (slot // share) * CAPACITY + mine_ref[0] * share + slot % share
     pick = ((places[0] == wanted) | (places[1] == wanted)).astype(f32).astype(bf16)
-    out_ref[...] = jnp.dot(pick, normed_ref[...], preferred_element_type=f32).astype(bf16)
+    picked = jnp.dot(pick, normed_ref[...], preferred_element_type=f32)
+    for j in range(pieces):
+        line_ref[pl.ds(j, slots, stride=pieces), :] = picked[:, j * LANES : (j + 1) * LANES]
+    out_ref[...] = line_ref[...].reshape(out_ref.shape).astype(bf16)
 
 
 def prepare_kernel(place_ref, weight_ref, hot_ref, column_ref):
@@ -186,10 +205,6 @@
     out_ref[...] = total.astype(jnp.bfloat16)
 
 
-def near(value):
-    return pltpu.with_memory_space_constraint(value, pltpu.VMEM)
-
-
 def route_experts(
     moe_rows, norm_gain, group_choice, member_choice, route_weight, w_gate, w_up, w_down, edge
 ):
@@ -205,15 +220,16 @@
         in_specs=[scalar, whole, whole, whole, whole],
         out_specs=[whole, whole],
         out_shape=[
-            pltpu.VMEM((slots, width), bf16),
+            jax.ShapeDtypeStruct((EXPERTS, share * width // LANES, LANES), bf16),
             pltpu.VMEM((TOP, tokens), jnp.int32),
         ],
-        scratch_shapes=[pltpu.VMEM((tokens, width), bf16)],
+        scratch_shapes=[
+            pltpu.VMEM((tokens, width), bf16),
+            pltpu.VMEM((slots * width // LANES, LANES), jnp.float32),
+        ],
         name="dispatch",
     )(mine, group_choice[None, :], member_choice.T, moe_rows, norm_gain[None, :])
-    incoming = lax.all_to_all(
-        outgoing.reshape(EXPERTS, share * width // LANES, LANES), "ep", 0, 0, tiled=True
-    )
+    incoming = lax.all_to_all(outgoing, "ep", 0, 0, tiled=True)
     hots, columns = pl.pallas_call(
         prepare_kernel,
         in_specs=[whole, whole],

time: 121 us -> 121 us (level)
  waiting for transfers between devices: 10.9 us -> 14.5 us
  Pallas kernels: 13.9 us -> 11 us
    pallas_call x1, Pallas kernels: 9.28 us -> 5.67 us  [attend_window(): pl.pallas_call(attention_kernel, in_specs=[scalar, scalar, whole, whole,...]
    all_to_all x1, waiting for transfers between devices: 4.28 us -> 7.87 us  [route_experts(): lax.all_to_all(produced.reshape(total // CAPACITY, CAPACITY, out_width),...]
  transfers between devices with their start and end apart: 3 -> 3, of which waited for: 3 -> 3; matrix products, arithmetic and copies ran while one was open for 3% -> 3% of each run, Pallas kernels for 9% -> 6%
where the time goes in v3:
time: 121 us; the launch traced here: 120 us
  blocking collectives  64.3 us (53%)
  starting transfers between devices  22.5 us (19%)
  waiting for transfers between devices  14.5 us (12%)
  Pallas kernels  11 us (9%)
  other arithmetic  2.6 us (2%)
  matrix products  2.6 us (2%)
  local copies, waits for them, and re-layouts  1.8 us (1%)
    all_gather x1, blocking collectives, route_experts(): lax.all_gather(hidden.astype(jnp.float16), 'tp', axis=0, tiled=False)  34.4 us
    all_gather x1, blocking collectives, route_experts(): block_rows = lax.all_gather(shared, 'tp', axis=0, tiled=True).astype(bf16)  30 us
    all_to_all x1, starting transfers between devices, route_experts(): incoming = lax.all_to_all(outgoing, 'ep', 0, 0, tiled=True)  13.2 us
    all_to_all x1, waiting for transfers between devices, route_experts(): lax.all_to_all(produced.reshape(total // CAPACITY, CAPACITY, out_width),...  7.87 us
    all_to_all x1, starting transfers between devices, route_experts(): lax.all_to_all(produced.reshape(total // CAPACITY, CAPACITY, out_width),...  7.38 us
    pallas_call x1, Pallas kernels, attend_window(): pl.pallas_call(attention_kernel, in_specs=[scalar, scalar, whole, whole,...  5.67 us
    all_to_all x1, waiting for transfers between devices, route_experts(): incoming = lax.all_to_all(outgoing, 'ep', 0, 0, tiled=True)  5.59 us
    pallas_call x1, Pallas kernels, route_experts(): pl.pallas_call(dispatch_kernel, in_specs=[scalar, whole, whole, whole, wh...  2.68 us
  transfers between devices with their start and end apart: 3, of which 3 were waited for; matrix products, arithmetic and copies ran while one was open for 3% of the time, Pallas kernels for 6%

profile of v3, /device:TPU:8, one launch (start us, length us, event | category | flops | bytes accessed | tf_op | source)
XLA Modules:
  0.0 120.1 jit_solution(6476788491905157192)
XLA Ops:
  0.6 2.7 %dispatch.1 = (bf16[32,32,128]{2,1,0:T(8,128)(2,1)}, s32[2,256]{1,0:T(2,128)S(1)}) custom-call(s32[1]{0:T(128)} %bitcast.1.mine_ref, s32[1,256]{1,0:T(1,128)} %bitcast.24, s32[2,256]{1,0:T(2,128)} %bitcast.22, bf16[256,2048]{1,0:T(8,128)(2,1)} %rows_ref.1, f32[1,2048]{1,0:T(1,128)} %bitcast.21), custom_call_target="tpu_custom_call" | custom-call | tf_op jit(solution)/shard_map/dispatch/pallas_call | solution.py:218
  3.3 0.0 copy-start.1
  3.3 13.2 %all-to-all-start = ((bf16[32,32,128]{2,1,0:T(8,128)(2,1)}), bf16[32,32,128]{2,1,0:T(8,128)(2,1)S(1)}, u32[]{:S(2)}, u32[]{:S(2)}) async-start(bf16[32,32,128]{2,1,0:T(8,128)(2,1)} %get-tuple-element.12), calls=%async_computation | async-start | bytes 524288 | tf_op jit(solution)/shard_map/all_to_all | solution.py:232
  16.5 0.9 slice.9
  17.4 1.9 %collective-permute-start = (bf16[2,128,256]{2,1,0:T(8,128)(2,1)S(1)}, bf16[2,128,256]{2,1,0:T(8,128)(2,1)S(1)}, u32[]{:S(2)}, u32[]{:S(2)}) collective-permute-start(bf16[2,128,256]{2,1,0:T(8,128)(2,1)S(1)} %slice.9), channel_id=1, source_target_pairs={{0,1},{1,2},{2,3},{3,4},{4,5},{5,6},{6,7},{7,8},{8,9},{9,10},{10,1... | collective-permute-start | bytes 393224 | tf_op jit(solution)/shard_map/ppermute | solution.py:102
  19.3 0.0 copy-done.1
  19.4 1.0 prepare.1
  20.3 2.3 %pad_maximum_fusion = bf16[2048,256]{1,0:T(8,128)(2,1)} fusion(bf16[2048,128]{1,0:T(8,128)(2,1)} %bitcast.19, bf16[2048,128]{1,0:T(8,128)(2,1)} %bitcast.20), kind=kLoop, calls=%fused_computation.5 | loop fusion | flops 2097152 | bytes 2097152 | tf_op jit(solution)/shard_map/concatenate | solution.py:243
  22.6 1.1 collective-permute-done.edge_ref
  23.7 5.6 %all-to-all-done = bf16[32,32,128]{2,1,0:T(8,128)(2,1)S(1)} async-done(((bf16[32,32,128]{2,1,0:T(8,128)(2,1)}), bf16[32,32,128]{2,1,0:T(8,128)(2,1)S(1)}, u32[]{:S(2)}, u32[]{:S(2)}) %all-to-all-start) | async-done | bytes 262176 | tf_op jit(solution)/shard_map/all_to_all | solution.py:232
  29.3 0.1 convert_element_type.32
  29.4 0.1 convert_element_type.33
  29.5 0.0 copy-start.3
  29.5 30.0 %all-gather.3 = f16[1024,2048]{1,0:T(8,128)(2,1)S(1)} all-gather(f16[64,2048]{1,0:T(8,128)(2,1)S(1)} %convert_element_type.33), channel_id=1, replica_groups=mesh['ep'=32,'tp'=16] {'tp'}, dimensions={0}, use_global_device_ids=true | all-gather | bytes 4456448 | tf_op jit(solution)/shard_map/all_gather | solution.py:248
  59.5 0.0 copy-done.3
  59.5 1.2 %fusion.2.y_ref = f32[1024,256]{1,0:T(8,128)S(1)} fusion(bf16[2048,256]{1,0:T(8,128)(2,1)S(1)} %copy-done.3, f16[1024,2048]{1,0:T(8,128)(2,1)S(1)} %all-gather.3), kind=kOutput, calls=%fused_computation.2 | convolution fusion | flops 1075838976 | bytes 6291456 | tf_op jit(solution)/shard_map/dot_general | solution.py:250
  60.7 0.0 copy-start.4
  60.7 0.6 hidden.1
  61.4 0.1 convert_element_type.35
  61.5 34.4 %all-gather.4 = f16[16640,128]{1,0:T(8,128)(2,1)S(1)} all-gather(f16[1040,128]{1,0:T(8,128)(2,1)S(1)} %convert_element_type.35), channel_id=2, replica_groups=mesh['ep'=32,'tp'=16] {'tp'}, dimensions={0}, use_global_device_ids=true | all-gather | bytes 4526080 | tf_op jit(solution)/shard_map/all_gather | solution.py:260
  95.8 0.2 fusion.10
  96.0 0.0 copy-done.4
  96.0 0.0 copy-start
  96.0 0.0 copy-start.2
  96.0 1.3 %fusion.4 = bf16[1040,128]{1,0:T(8,128)(2,1)S(1)} fusion(f16[16,1040,128]{2,1,0:T(8,128)(2,1)S(1)} %bitcast.18, bf16[16,128,128]{2,1,0:T(8,128)(2,1)S(1)} %bitcast.25, f32[16]{0:T(128)S(1)} %fusion.10), kind=kOutput, calls=%fused_computation.4 | convolution fusion | flops 548175872 | bytes 5050432 | tf_op jit(solution)/shard_map/trk,tko->ro/dot_general | solution.py:267
  97.4 0.7 slice.20
  98.1 7.4 %all-to-all-start.1 = ((bf16[32,32,128]{2,1,0:T(8,128)(2,1)}), bf16[32,32,128]{2,1,0:T(8,128)(2,1)S(1)}, u32[]{:S(2)}, u32[]{:S(2)}) async-start(bf16[32,32,128]{2,1,0:T(8,128)(2,1)} %bitcast.11), calls=%async_computation.1 | async-start | bytes 524288 | tf_op jit(solution)/shard_map/all_to_all | solution.py:273
  105.5 0.0 copy-done
  105.5 0.0 copy-done.2
  105.5 5.7 %attention.1 = bf16[384,1024]{1,0:T(8,128)(2,1)} custom-call(s32[1]{0:T(128)} %bitcast.first_ref, f32[16]{0:T(128)} %sink_ref, bf16[384,1024]{1,0:T(8,128)(2,1)S(1)} %copy-done.2, bf16[2,384,256]{2,1,0:T(8,128)(2,1)S(1)} %copy-done, bf16[2,128,256]{2,1,0:T(8,128)(2,1)S(1)} %collective-permute-done.edge_ref), custom_call_target="tpu_custom_call" | custom-call | flops 3000000000 | bytes 3000000 | tf_op jit(solution)/shard_map/attention/pallas_call | solution.py:110
  111.2 7.9 %all-to-all-done.1 = bf16[32,32,128]{2,1,0:T(8,128)(2,1)S(1)} async-done(((bf16[32,32,128]{2,1,0:T(8,128)(2,1)}), bf16[32,32,128]{2,1,0:T(8,128)(2,1)S(1)}, u32[]{:S(2)}, u32[]{:S(2)}) %all-to-all-start.1) | async-done | bytes 262176 | tf_op jit(solution)/shard_map/all_to_all | solution.py:273
  119.1 1.1 combine.1
Async XLA Ops:
  3.3 16.0 %copy-start.1 = (s32[2,256]{1,0:T(2,128)}, s32[2,256]{1,0:T(2,128)S(1)}, u32[]{:S(2)}) copy-start(s32[2,256]{1,0:T(2,128)S(1)} %get-tuple-element.13.place_ref) | copy-start | bytes 6148
  3.3 26.0 %all-to-all-start = ((bf16[32,32,128]{2,1,0:T(8,128)(2,1)}), bf16[32,32,128]{2,1,0:T(8,128)(2,1)S(1)}, u32[]{:S(2)}, u32[]{:S(2)}) async-start(bf16[32,32,128]{2,1,0:T(8,128)(2,1)} %get-tuple-element.12), calls=%async_computation | async-start | bytes 524288 | tf_op jit(solution)/shard_map/all_to_all | solution.py:232
  17.4 6.3 %collective-permute-start = (bf16[2,128,256]{2,1,0:T(8,128)(2,1)S(1)}, bf16[2,128,256]{2,1,0:T(8,128)(2,1)S(1)}, u32[]{:S(2)}, u32[]{:S(2)}) collective-permute-start(bf16[2,128,256]{2,1,0:T(8,128)(2,1)S(1)} %slice.9), channel_id=1, source_target_pairs={{0,1},{1,2},{2,3},{3,4},{4,5},{5,6},{6,7},{7,8},{8,9},{9,10},{10,1... | collective-permute-start | bytes 393224 | tf_op jit(solution)/shard_map/ppermute | solution.py:102
  29.5 30.0 %copy-start.3 = (bf16[2048,256]{1,0:T(8,128)(2,1)S(1)}, bf16[2048,256]{1,0:T(8,128)(2,1)}, u32[]{:S(2)}) copy-start(bf16[2048,256]{1,0:T(8,128)(2,1)} %pad_maximum_fusion) | copy-start | bytes 3145732
  60.7 35.3 %copy-start.4 = (bf16[1,2048,128]{2,1,0:T(8,128)(2,1)S(1)}, bf16[1,2048,128]{2,1,0:T(8,128)(2,1)}, u32[]{:S(2)}) copy-start(bf16[1,2048,128]{2,1,0:T(8,128)(2,1)} %param.21) | copy-start | bytes 1572868
  96.0 9.5 %copy-start = (bf16[2,384,256]{2,1,0:T(8,128)(2,1)S(1)}, bf16[2,384,256]{2,1,0:T(8,128)(2,1)}, u32[]{:S(2)}) copy-start(bf16[2,384,256]{2,1,0:T(8,128)(2,1)} %kv_ref.1) | copy-start | bytes 1179652
  96.0 9.5 %copy-start.2 = (bf16[384,1024]{1,0:T(8,128)(2,1)S(1)}, bf16[384,1024]{1,0:T(8,128)(2,1)}, u32[]{:S(2)}) copy-start(bf16[384,1024]{1,0:T(8,128)(2,1)} %q_ref.1) | copy-start | bytes 2359300
  98.1 21.0 %all-to-all-start.1 = ((bf16[32,32,128]{2,1,0:T(8,128)(2,1)}), bf16[32,32,128]{2,1,0:T(8,128)(2,1)S(1)}, u32[]{:S(2)}, u32[]{:S(2)}) async-start(bf16[32,32,128]{2,1,0:T(8,128)(2,1)} %bitcast.11), calls=%async_computation.1 | async-start | bytes 524288 | tf_op jit(solution)/shard_map/all_to_all | solution.py:273

commit v4 on v3

--- a/solution.py
+++ b/solution.py
@@ -5,7 +5,7 @@
 from jax.experimental.pallas import tpu as pltpu
 from jax.sharding import PartitionSpec as P
 
-QH = 16
+
 KVH = 4
 HD = 64
 WINDOW = 128
@@ -95,11 +95,10 @@
                 ).astype(bf16)
 
 
-def edge_of(keys_values):
-    length = keys_values.shape[1]
+def passed_along(value):
     peers = lax.axis_size(("ep", "tp"))
     pairs = [(i, i + 1) for i in range(peers - 1)]
-    return lax.ppermute(keys_values[:, length - WINDOW :, :], ("ep", "tp"), pairs)
+    return lax.ppermute(value, ("ep", "tp"), pairs)
 
 
 def attend_window(queries, keys_values, sink_logits, edge):
@@ -152,7 +151,14 @@
     out_ref[...] = line_ref[...].reshape(out_ref.shape).astype(bf16)
 
 
-def prepare_kernel(place_ref, weight_ref, hot_ref, column_ref):
+def prepare_kernel(
+    place_ref, weight_ref, gate_ref, up_ref, hot_ref, column_ref, both_ref, gate_sem, up_sem
+):
+    units = gate_ref.shape[1]
+    gate_copy = pltpu.make_async_copy(gate_ref, both_ref.at[:, :units], gate_sem)
+    up_copy = pltpu.make_async_copy(up_ref, both_ref.at[:, units:], up_sem)
+    gate_copy.start()
+    up_copy.start()
     f32 = jnp.float32
     bf16 = jnp.bfloat16
     tokens = place_ref.shape[1]
@@ -164,6 +170,8 @@
             slot = lax.broadcasted_iota(jnp.int32, (tokens, LANES), 1) + j * LANES
             hot_ref[k, :, j * LANES : (j + 1) * LANES] = (place == slot).astype(f32).astype(bf16)
         column_ref[k] = jnp.broadcast_to(weight_ref[k : k + 1, :], (LANES, tokens)).T
+    gate_copy.wait()
+    up_copy.wait()
 
 
 def hidden_kernel(y_ref, out_ref, plain_ref, ordered_ref):
@@ -206,7 +214,7 @@
 
 
 def route_experts(
-    moe_rows, norm_gain, group_choice, member_choice, route_weight, w_gate, w_up, w_down, edge
+    moe_rows, norm_gain, group_choice, member_choice, route_weight, w_gate, w_up, w_down
 ):
     bf16 = jnp.bfloat16
     tokens, width = moe_rows.shape
@@ -215,6 +223,7 @@
     mine = lax.axis_index("tp").astype(jnp.int32).reshape(1)
     whole = pl.BlockSpec(memory_space=pltpu.VMEM)
     scalar = pl.BlockSpec(memory_space=pltpu.SMEM)
+    outside = pl.BlockSpec(memory_space=pl.ANY)
     outgoing, places = pl.pallas_call(
         dispatch_kernel,
         in_specs=[scalar, whole, whole, whole, whole],
@@ -230,20 +239,19 @@
         name="dispatch",
     )(mine, group_choice[None, :], member_choice.T, moe_rows, norm_gain[None, :])
     incoming = lax.all_to_all(outgoing, "ep", 0, 0, tiled=True)
-    hots, columns = pl.pallas_call(
+    hots, columns, both = pl.pallas_call(
         prepare_kernel,
-        in_specs=[whole, whole],
-        out_specs=[whole, whole],
+        in_specs=[whole, whole, outside, outside],
+        out_specs=[whole, whole, whole],
         out_shape=[
             pltpu.VMEM((TOP, tokens, EXPERTS * CAPACITY), bf16),
             pltpu.VMEM((TOP, tokens, LANES), jnp.float32),
+            pltpu.VMEM((width, 2 * w_gate.shape[2]), bf16),
         ],
+        scratch_shapes=[pltpu.SemaphoreType.DMA, pltpu.SemaphoreType.DMA],
         name="prepare",
-    )(places, route_weight.T)
-    both = jnp.concatenate([w_gate[0], w_up[0]], axis=1)
-    incoming, edge, hots, columns, both = lax.optimization_barrier(
-        (incoming, edge, hots, columns, both)
-    )
+    )(near(places), route_weight.T, w_gate[0], w_up[0])
+    incoming, hots, columns, both = lax.optimization_barrier((incoming, hots, columns, both))
     shared = incoming.reshape(slots, width).astype(jnp.float16)
     block_rows = lax.all_gather(shared, "tp", axis=0, tiled=True).astype(bf16)
     total = block_rows.shape[0]
@@ -266,10 +274,10 @@
     weight = w_down[0].reshape(TP, units, out_width).astype(jnp.float32) * factor[:, None, None]
     produced = jnp.einsum(
         "trk,tko->ro",
-        spread.astype(bf16),
+        spread[:, :total].astype(bf16),
         weight.astype(bf16),
         preferred_element_type=jnp.float32,
-    ).astype(bf16)[:total]
+    ).astype(bf16)
     returned = lax.all_to_all(
         produced.reshape(total // CAPACITY, CAPACITY, out_width), "ep", 0, 0, tiled=True
     )
@@ -280,7 +288,7 @@
         out_shape=jax.ShapeDtypeStruct((tokens, out_width), bf16),
         name="combine",
     )(near(hots), near(columns), near(returned.reshape(EXPERTS * CAPACITY, out_width)))
-    return mixed, edge, produced
+    return mixed, produced
 
 
 def shards(
@@ -296,8 +304,8 @@
     w_up,
     w_down,
 ):
-    edge = edge_of(keys_values)
-    mixed, edge, produced = route_experts(
+    edge = passed_along(keys_values[:, keys_values.shape[1] - WINDOW :, :])
+    mixed, produced = route_experts(
         moe_rows,
         norm_gain,
         group_choice,
@@ -306,7 +314,6 @@
         w_gate,
         w_up,
         w_down,
-        edge,
     )
     sink_logits, produced = lax.optimization_barrier((sink_logits, produced))
     attended = attend_window(queries, keys_values, sink_logits, edge)

time: 121 us -> 121 us (level)
  the two profiles are of different devices: /device:TPU:8 before, /device:TPU:64 now
where the time goes in v4:
time: 121 us; the launch traced here: 120 us
  blocking collectives  64.7 us (53%)
  starting transfers between devices  19.7 us (16%)
  waiting for transfers between devices  19.4 us (16%)
  Pallas kernels  12.1 us (10%)
  matrix products  3.28 us (3%)
    all_gather x1, blocking collectives, route_experts(): lax.all_gather(hidden.astype(jnp.float16), 'tp', axis=0, tiled=False)  32.4 us
    all_gather x1, blocking collectives, route_experts(): block_rows = lax.all_gather(shared, 'tp', axis=0, tiled=True).astype(bf16)  32.3 us
    all_to_all x1, starting transfers between devices, route_experts(): incoming = lax.all_to_all(outgoing, 'ep', 0, 0, tiled=True)  12.6 us
    all_to_all x1, waiting for transfers between devices, route_experts(): incoming = lax.all_to_all(outgoing, 'ep', 0, 0, tiled=True)  10.2 us
    ppermute x1, waiting for transfers between devices, passed_along(): return lax.ppermute(value, ('ep', 'tp'), pairs)  9.19 us
    pallas_call x1, Pallas kernels, attend_window(): pl.pallas_call(attention_kernel, in_specs=[scalar, scalar, whole, whole,...  5.8 us
    all_to_all x1, starting transfers between devices, route_experts(): lax.all_to_all(produced.reshape(total // CAPACITY, CAPACITY, out_width),...  5.15 us
    pallas_call x1, Pallas kernels, route_experts(): pl.pallas_call(dispatch_kernel, in_specs=[scalar, whole, whole, whole, wh...  2.68 us
  transfers between devices with their start and end apart: 3, of which 2 were waited for; matrix products, arithmetic and copies ran while one was open for 0% of the time, Pallas kernels for 6%

profile of v4, /device:TPU:64, one launch (start us, length us, event | category | flops | bytes accessed | tf_op | source)
XLA Modules:
  0.0 120.4 jit_solution(740576620254060179)
XLA Ops:
  0.6 2.7 %dispatch.1 = (bf16[32,32,128]{2,1,0:T(8,128)(2,1)}, s32[2,256]{1,0:T(2,128)S(1)}) custom-call(s32[1]{0:T(128)} %bitcast.1.mine_ref, s32[1,256]{1,0:T(1,128)} %bitcast.26, s32[2,256]{1,0:T(2,128)} %bitcast.24, bf16[256,2048]{1,0:T(8,128)(2,1)} %rows_ref.1, f32[1,2048]{1,0:T(1,128)} %bitcast.23), custom_call_target="tpu_custom_call" | custom-call | tf_op jit(solution)/shard_map/dispatch/pallas_call | solution.py:227
  3.3 12.6 %all-to-all-start = ((bf16[32,32,128]{2,1,0:T(8,128)(2,1)}), bf16[32,32,128]{2,1,0:T(8,128)(2,1)S(1)}, u32[]{:S(2)}, u32[]{:S(2)}) async-start(bf16[32,32,128]{2,1,0:T(8,128)(2,1)} %get-tuple-element.12), calls=%async_computation | async-start | bytes 524288 | tf_op jit(solution)/shard_map/all_to_all | solution.py:241
  15.9 1.9 %prepare.1 = (bf16[2,256,1024]{2,1,0:T(8,128)(2,1)S(1)}, f32[2,256,128]{2,1,0:T(8,128)S(1)}, bf16[2048,256]{1,0:T(8,128)(2,1)S(1)}) custom-call(s32[2,256]{1,0:T(2,128)S(1)} %get-tuple-element.13.place_ref, f32[2,256]{1,0:T(2,128)} %bitcast.25, bf16[2048,128]{1,0:T(8,128)(2,1)} %bitcast.21, bf16[2048,128]{1,0:T(8,128)(2,1)} %bitcast.22), custom_call_target="tpu_custom_call" | custom-call | tf_op jit(solution)/shard_map/prepare/pallas_call | solution.py:242
  17.8 0.0 copy-start
  17.8 10.2 %all-to-all-done = bf16[32,32,128]{2,1,0:T(8,128)(2,1)S(1)} async-done(((bf16[32,32,128]{2,1,0:T(8,128)(2,1)}), bf16[32,32,128]{2,1,0:T(8,128)(2,1)S(1)}, u32[]{:S(2)}, u32[]{:S(2)}) %all-to-all-start) | async-done | bytes 262176 | tf_op jit(solution)/shard_map/all_to_all | solution.py:241
  28.1 0.1 convert_element_type.32
  28.1 0.1 convert_element_type.33
  28.3 0.0 copy-done
  28.3 32.3 %all-gather.3 = f16[1024,2048]{1,0:T(8,128)(2,1)S(1)} all-gather(f16[64,2048]{1,0:T(8,128)(2,1)S(1)} %convert_element_type.33), channel_id=1, replica_groups=mesh['ep'=32,'tp'=16] {'tp'}, dimensions={0}, use_global_device_ids=true | all-gather | bytes 4456448 | tf_op jit(solution)/shard_map/all_gather | solution.py:256
  60.6 1.2 %fusion.1.y_ref = f32[1024,256]{1,0:T(8,128)S(1)} fusion(bf16[2048,256]{1,0:T(8,128)(2,1)S(1)} %get-tuple-element.18, f16[1024,2048]{1,0:T(8,128)(2,1)S(1)} %all-gather.3), kind=kOutput, calls=%fused_computation.2 | convolution fusion | flops 1075838976 | bytes 6291456 | tf_op jit(solution)/shard_map/dot_general | solution.py:258
  61.8 0.6 hidden.1
  62.5 0.0 copy-start.4
  62.5 0.1 convert_element_type.35
  62.6 32.4 %all-gather.4 = f16[16640,128]{1,0:T(8,128)(2,1)S(1)} all-gather(f16[1040,128]{1,0:T(8,128)(2,1)S(1)} %convert_element_type.35), channel_id=2, replica_groups=mesh['ep'=32,'tp'=16] {'tp'}, dimensions={0}, use_global_device_ids=true | all-gather | bytes 4526080 | tf_op jit(solution)/shard_map/all_gather | solution.py:268
  95.0 0.2 fusion.8
  95.2 0.0 copy-done.4
  95.2 0.0 copy-start.2
  95.2 0.0 copy-start.3
  95.2 2.0 %fusion.4 = bf16[1024,128]{1,0:T(8,128)(2,1)} fusion(f16[16,1040,128]{2,1,0:T(8,128)(2,1)S(1)} %bitcast.20, bf16[16,128,128]{2,1,0:T(8,128)(2,1)S(1)} %bitcast.27, f32[16]{0:T(128)S(1)} %fusion.8), kind=kOutput, calls=%fused_computation.5 | convolution fusion | flops 539885568 | bytes 4981248 | tf_op jit(solution)/shard_map/trk,tko->ro/dot_general | solution.py:275
  97.2 5.1 %all-to-all-start.1 = ((bf16[32,32,128]{2,1,0:T(8,128)(2,1)}), bf16[32,32,128]{2,1,0:T(8,128)(2,1)S(1)}, u32[]{:S(2)}, u32[]{:S(2)}) async-start(bf16[32,32,128]{2,1,0:T(8,128)(2,1)} %bitcast.11), calls=%async_computation.1 | async-start | bytes 524288 | tf_op jit(solution)/shard_map/all_to_all | solution.py:281
  102.4 0.0 copy-done.2
  102.4 1.9 %collective-permute-start = (bf16[2,128,256]{2,1,0:T(8,128)(2,1)S(1)}, bf16[2,128,256]{2,1,0:T(8,128)(2,1)S(1)}, u32[]{:S(2)}, u32[]{:S(2)}) collective-permute-start(bf16[2,128,256]{2,1,0:T(8,128)(2,1)S(1)} %slice.11), channel_id=1, source_target_pairs={{0,1},{1,2},{2,3},{3,4},{4,5},{5,6},{6,7},{7,8},{8,9},{9,10},{10,1... | collective-permute-start | bytes 393224 | tf_op jit(solution)/shard_map/ppermute | solution.py:101
  104.3 9.2 %collective-permute-done.edge_ref = bf16[2,128,256]{2,1,0:T(8,128)(2,1)S(1)} collective-permute-done((bf16[2,128,256]{2,1,0:T(8,128)(2,1)S(1)}, bf16[2,128,256]{2,1,0:T(8,128)(2,1)S(1)}, u32[]{:S(2)}, u32[]{:S(2)}) %collective-permute-start) | collective-permute-done | bytes 131104 | tf_op jit(solution)/shard_map/ppermute | solution.py:101
  113.5 0.0 copy-done.3
  113.5 0.0 copy-start.1
  113.5 5.8 %attention.1 = bf16[384,1024]{1,0:T(8,128)(2,1)} custom-call(s32[1]{0:T(128)} %bitcast.first_ref, f32[16]{0:T(128)} %sink_ref, bf16[384,1024]{1,0:T(8,128)(2,1)S(1)} %copy-done.3, bf16[2,384,256]{2,1,0:T(8,128)(2,1)S(1)} %copy-done.2, bf16[2,128,256]{2,1,0:T(8,128)(2,1)S(1)} %collective-permute-done.edge_ref), custom_call_target="tpu_custom_call" | custom-call | flops 3000000000 | bytes 3000000 | tf_op jit(solution)/shard_map/attention/pallas_call | solution.py:109
  119.3 0.0 all-to-all-done.1
  119.3 0.0 copy-done.1
  119.4 1.1 combine.1
  (1 shorter events, 0.0 us)
Async XLA Ops:
  3.3 24.8 %all-to-all-start = ((bf16[32,32,128]{2,1,0:T(8,128)(2,1)}), bf16[32,32,128]{2,1,0:T(8,128)(2,1)S(1)}, u32[]{:S(2)}, u32[]{:S(2)}) async-start(bf16[32,32,128]{2,1,0:T(8,128)(2,1)} %get-tuple-element.12), calls=%async_computation | async-start | bytes 524288 | tf_op jit(solution)/shard_map/all_to_all | solution.py:241
  17.8 10.5 %copy-start = (f32[2,256,128]{2,1,0:T(8,128)}, f32[2,256,128]{2,1,0:T(8,128)S(1)}, u32[]{:S(2)}) copy-start(f32[2,256,128]{2,1,0:T(8,128)S(1)} %get-tuple-element.21.column_ref) | copy-start | bytes 786436
  62.5 32.7 %copy-start.4 = (bf16[1,2048,128]{2,1,0:T(8,128)(2,1)S(1)}, bf16[1,2048,128]{2,1,0:T(8,128)(2,1)}, u32[]{:S(2)}) copy-start(bf16[1,2048,128]{2,1,0:T(8,128)(2,1)} %param.21) | copy-start | bytes 1572868
  95.2 7.2 %copy-start.2 = (bf16[2,384,256]{2,1,0:T(8,128)(2,1)S(1)}, bf16[2,384,256]{2,1,0:T(8,128)(2,1)}, u32[]{:S(2)}) copy-start(bf16[2,384,256]{2,1,0:T(8,128)(2,1)} %kv_ref.1) | copy-start | bytes 1179652
  95.2 18.4 %copy-start.3 = (bf16[384,1024]{1,0:T(8,128)(2,1)S(1)}, bf16[384,1024]{1,0:T(8,128)(2,1)}, u32[]{:S(2)}) copy-start(bf16[384,1024]{1,0:T(8,128)(2,1)} %q_ref.1) | copy-start | bytes 2359300
  97.2 22.1 %all-to-all-start.1 = ((bf16[32,32,128]{2,1,0:T(8,128)(2,1)}), bf16[32,32,128]{2,1,0:T(8,128)(2,1)S(1)}, u32[]{:S(2)}, u32[]{:S(2)}) async-start(bf16[32,32,128]{2,1,0:T(8,128)(2,1)} %bitcast.11), calls=%async_computation.1 | async-start | bytes 524288 | tf_op jit(solution)/shard_map/all_to_all | solution.py:281
  102.4 11.1 %collective-permute-start = (bf16[2,128,256]{2,1,0:T(8,128)(2,1)S(1)}, bf16[2,128,256]{2,1,0:T(8,128)(2,1)S(1)}, u32[]{:S(2)}, u32[]{:S(2)}) collective-permute-start(bf16[2,128,256]{2,1,0:T(8,128)(2,1)S(1)} %slice.11), channel_id=1, source_target_pairs={{0,1},{1,2},{2,3},{3,4},{4,5},{5,6},{6,7},{7,8},{8,9},{9,10},{10,1... | collective-permute-start | bytes 393224 | tf_op jit(solution)/shard_map/ppermute | solution.py:101
  113.5 5.8 %copy-start.1 = (f32[2,256,128]{2,1,0:T(8,128)S(1)}, f32[2,256,128]{2,1,0:T(8,128)}, u32[]{:S(2)}) copy-start(f32[2,256,128]{2,1,0:T(8,128)} %copy-done) | copy-start | bytes 786436

commit v5 on v4

--- a/solution.py
+++ b/solution.py
@@ -23,10 +23,11 @@
     return pltpu.with_memory_space_constraint(value, pltpu.VMEM)
 
 
-def attention_kernel(first_ref, sink_ref, q_ref, kv_ref, edge_ref, out_ref, band_ref):
+def attend_blocks(
+    begin, blocks, first_ref, sink_ref, q_ref, kv_ref, edge_ref, out_ref, band_ref, done_ref, copy_sem
+):
     f32 = jnp.float32
     bf16 = jnp.bfloat16
-    blocks = q_ref.shape[0] // WINDOW
     row = lax.broadcasted_iota(jnp.int32, (WINDOW, WINDOW), 0)
     col = lax.broadcasted_iota(jnp.int32, (WINDOW, WINDOW), 1)
     causal = col <= row
@@ -36,10 +37,11 @@
         for part in range(blocks + 1):
             for h in range(KVH // 2):
                 lanes = slice(h * LANES, (h + 1) * LANES)
-                if part == 0:
+                if part == 0 and edge_ref is not None:
                     value = edge_ref[which, :, lanes]
                 else:
-                    value = kv_ref[which, (part - 1) * WINDOW : part * WINDOW, lanes]
+                    at = begin + part - 1
+                    value = kv_ref[which, at * WINDOW : (at + 1) * WINDOW, lanes]
                 if which == 0:
                     value = value * bf16(HD ** (-0.5))
                 turned = pltpu.roll(value.astype(f32), HD, 1).astype(bf16)
@@ -49,8 +51,9 @@
                 band_ref[which, 2 * h + 1, 0, at, :] = jnp.where(low, turned, zero)
                 band_ref[which, 2 * h + 1, 1, at, :] = jnp.where(low, zero, value)
 
-    absent = jnp.where(first_ref[0] == 1, f32(-1e30), f32(0.0))
-    bias = jnp.where(causal, f32(0.0), absent)
+    if edge_ref is not None:
+        absent = jnp.where(first_ref[0] == 1, f32(-1e30), f32(0.0))
+        bias = jnp.where(causal, f32(0.0), absent)
     for block in range(blocks):
         start = block * WINDOW
         band = pl.ds(start, 2 * WINDOW)
@@ -58,7 +61,7 @@
             keys = jnp.concatenate([band_ref[0, c, 0, band, :], band_ref[0, c, 1, band, :]], axis=0)
             values = jnp.concatenate([band_ref[1, c, 0, band, :], band_ref[1, c, 1, band, :]], axis=0)
             q = jnp.concatenate(
-                [q_ref[pl.ds(start, WINDOW), c * 256 + p * LANES : c * 256 + (p + 1) * LANES] for p in range(2)],
+                [q_ref[pl.ds(begin * WINDOW + start, WINDOW), c * 256 + p * LANES : c * 256 + (p + 1) * LANES] for p in range(2)],
                 axis=0,
             )
             scores = lax.dot_general(q, keys, (((1,), (1,)), ((), ())), preferred_element_type=f32)
@@ -74,7 +77,7 @@
                     s_prev = scores[p * WINDOW : (p + 1) * WINDOW, base : base + WINDOW]
                     s_cur = scores[p * WINDOW : (p + 1) * WINDOW, base + WINDOW : base + 2 * WINDOW]
                     s = jnp.where(causal, s_cur, s_prev)
-                    if block == 0:
+                    if edge_ref is not None and block == 0:
                         s = s + bias
                     highest = jnp.maximum(jnp.max(s, axis=1, keepdims=True), sink_ref[head + side])
                     w = jnp.exp(s - highest)
@@ -90,9 +93,25 @@
             summed = jnp.dot(jnp.concatenate(lines, axis=0), values, preferred_element_type=f32)
             for p in range(2):
                 at = c * 256 + p * LANES
-                out_ref[pl.ds(start, WINDOW), at : at + LANES] = (
+                done_ref[pl.ds(start, WINDOW), at : at + LANES] = (
                     summed[p * WINDOW : (p + 1) * WINDOW] / totals[p]
                 ).astype(bf16)
+    copy = pltpu.make_async_copy(
+        done_ref, out_ref.at[begin * WINDOW : (begin + blocks) * WINDOW, :], copy_sem
+    )
+    copy.start()
+    copy.wait()
+
+
+def later_blocks_kernel(sink_ref, q_ref, kv_ref, out_ref, band_ref, done_ref, copy_sem):
+    blocks = q_ref.shape[0] // WINDOW - 1
+    attend_blocks(1, blocks, None, sink_ref, q_ref, kv_ref, None, out_ref, band_ref, done_ref, copy_sem)
+
+
+def first_block_kernel(
+    first_ref, sink_ref, q_ref, kv_ref, edge_ref, kept_ref, out_ref, band_ref, done_ref, copy_sem
+):
+    attend_blocks(0, 1, first_ref, sink_ref, q_ref, kv_ref, edge_ref, out_ref, band_ref, done_ref, copy_sem)
 
 
 def passed_along(value):
@@ -105,16 +124,39 @@
     first = (lax.axis_index(("ep", "tp")) == 0).astype(jnp.int32).reshape(1)
     whole = pl.BlockSpec(memory_space=pltpu.VMEM)
     scalar = pl.BlockSpec(memory_space=pltpu.SMEM)
-    rows = keys_values.shape[1] + WINDOW
+    outside = pl.BlockSpec(memory_space=pl.ANY)
+    width = queries.shape[1]
+    blocks = queries.shape[0] // WINDOW
+    queries = near(queries)
+    keys_values = near(keys_values)
+
+    def scratch(count):
+        return [
+            pltpu.VMEM((2, KVH, 2, (count + 1) * WINDOW, LANES), jnp.bfloat16),
+            pltpu.VMEM((count * WINDOW, width), jnp.bfloat16),
+            pltpu.SemaphoreType.DMA,
+        ]
+
+    result = jax.ShapeDtypeStruct(queries.shape, jnp.bfloat16)
+    later = pl.pallas_call(
+        later_blocks_kernel,
+        in_specs=[scalar, whole, whole],
+        out_specs=outside,
+        out_shape=result,
+        scratch_shapes=scratch(blocks - 1),
+        cost_estimate=pl.CostEstimate(flops=2 * 10**9, bytes_accessed=2 * 10**6, transcendentals=10**6),
+        name="later_blocks",
+    )(sink_logits, queries, keys_values)
     return pl.pallas_call(
-        attention_kernel,
-        in_specs=[scalar, scalar, whole, whole, whole],
-        out_specs=whole,
-        out_shape=jax.ShapeDtypeStruct(queries.shape, jnp.bfloat16),
-        scratch_shapes=[pltpu.VMEM((2, KVH, 2, rows, LANES), jnp.bfloat16)],
-        cost_estimate=pl.CostEstimate(flops=3 * 10**9, bytes_accessed=3 * 10**6, transcendentals=10**6),
-        name="attention",
-    )(first, sink_logits, near(queries), near(keys_values), near(edge))
+        first_block_kernel,
+        in_specs=[scalar, scalar, whole, whole, whole, outside],
+        out_specs=outside,
+        out_shape=result,
+        scratch_shapes=scratch(1),
+        input_output_aliases={5: 0},
+        cost_estimate=pl.CostEstimate(flops=10**9, bytes_accessed=10**6, transcendentals=10**6),
+        name="first_block",
+    )(first, sink_logits, queries, keys_values, near(edge), later)
 
 
 def dispatch_kernel(mine_ref, group_ref, member_ref, rows_ref, gain_ref, out_ref, place_ref, normed_ref, line_ref):
@@ -214,7 +256,7 @@
 
 
 def route_experts(
-    moe_rows, norm_gain, group_choice, member_choice, route_weight, w_gate, w_up, w_down
+    moe_rows, norm_gain, group_choice, member_choice, route_weight, w_gate, w_up, w_down, last_rows
 ):
     bf16 = jnp.bfloat16
     tokens, width = moe_rows.shape
@@ -251,7 +293,9 @@
         scratch_shapes=[pltpu.SemaphoreType.DMA, pltpu.SemaphoreType.DMA],
         name="prepare",
     )(near(places), route_weight.T, w_gate[0], w_up[0])
-    incoming, hots, columns, both = lax.optimization_barrier((incoming, hots, columns, both))
+    incoming, last_rows, hots, columns, both = lax.optimization_barrier(
+        (incoming, last_rows, hots, columns, both)
+    )
     shared = incoming.reshape(slots, width).astype(jnp.float16)
     block_rows = lax.all_gather(shared, "tp", axis=0, tiled=True).astype(bf16)
     total = block_rows.shape[0]
@@ -288,7 +332,7 @@
         out_shape=jax.ShapeDtypeStruct((tokens, out_width), bf16),
         name="combine",
     )(near(hots), near(columns), near(returned.reshape(EXPERTS * CAPACITY, out_width)))
-    return mixed, produced
+    return mixed, last_rows, produced
 
 
 def shards(
@@ -304,8 +348,8 @@
     w_up,
     w_down,
 ):
-    edge = passed_along(keys_values[:, keys_values.shape[1] - WINDOW :, :])
-    mixed, produced = route_experts(
+    last_rows = keys_values[:, keys_values.shape[1] - WINDOW :, :]
+    mixed, last_rows, produced = route_experts(
         moe_rows,
         norm_gain,
         group_choice,
@@ -314,8 +358,10 @@
         w_gate,
         w_up,
         w_down,
-    )
-    sink_logits, produced = lax.optimization_barrier((sink_logits, produced))
+        last_rows,
+    )
+    last_rows, sink_logits, produced = lax.optimization_barrier((last_rows, sink_logits, produced))
+    edge = passed_along(last_rows)
     attended = attend_window(queries, keys_values, sink_logits, edge)
     return (attended, mixed)
 

time: 121 us -> 118 us (0.975)
  waiting for transfers between devices: 19.4 us -> 14.2 us
  Pallas kernels: 12.1 us -> 13.5 us
    ppermute x1, waiting for transfers between devices: 9.19 us -> 4.89 us  [passed_along(): return lax.ppermute(value, ('ep', 'tp'), pairs)]
    pallas_call x1 -> x2, Pallas kernels: 5.8 us -> 7.26 us  [the longest x1 4.3 us: attend_window(): pl.pallas_call(later_blocks_kernel, in_specs=[scalar, whole, whole], out_...]
  transfers between devices with their start and end apart: 3 -> 3, of which waited for: 2 -> 2; matrix products, arithmetic and copies ran while one was open for 0% -> 1% of each run, Pallas kernels for 6% -> 8%
where the time goes in v5:
time: 118 us
  blocking collectives  64.7 us (55%)
  starting transfers between devices  19.8 us (17%)
  waiting for transfers between devices  14.2 us (12%)
  Pallas kernels  13.5 us (11%)
  matrix products  3.28 us (3%)
    all_gather x1, blocking collectives, route_experts(): lax.all_gather(hidden.astype(jnp.float16), 'tp', axis=0, tiled=False)  32.4 us
    all_gather x1, blocking collectives, route_experts(): block_rows = lax.all_gather(shared, 'tp', axis=0, tiled=True).astype(bf16)  32.3 us
    all_to_all x1, starting transfers between devices, route_experts(): incoming = lax.all_to_all(outgoing, 'ep', 0, 0, tiled=True)  12.6 us
    all_to_all x1, waiting for transfers between devices, route_experts(): incoming = lax.all_to_all(outgoing, 'ep', 0, 0, tiled=True)  9.32 us
    all_to_all x1, starting transfers between devices, route_experts(): lax.all_to_all(produced.reshape(total // CAPACITY, CAPACITY, out_width),...  5.15 us
    ppermute x1, waiting for transfers between devices, passed_along(): return lax.ppermute(value, ('ep', 'tp'), pairs)  4.89 us
    pallas_call x1, Pallas kernels, attend_window(): pl.pallas_call(later_blocks_kernel, in_specs=[scalar, whole, whole], out_...  4.3 us
    pallas_call x1, Pallas kernels, attend_window(): pl.pallas_call(first_block_kernel, in_specs=[scalar, scalar, whole, whole...  2.97 us
  transfers between devices with their start and end apart: 3, of which 2 were waited for; matrix products, arithmetic and copies ran while one was open for 1% of the time, Pallas kernels for 8%

profile of v5, /device:TPU:64, one launch (start us, length us, event | category | flops | bytes accessed | tf_op | source)
XLA Modules:
  0.0 117.7 jit_solution(2312919652393225958)
XLA Ops:
  0.6 2.7 %dispatch.1 = (bf16[32,32,128]{2,1,0:T(8,128)(2,1)}, s32[2,256]{1,0:T(2,128)S(1)}) custom-call(s32[1]{0:T(128)} %bitcast.1.mine_ref, s32[1,256]{1,0:T(1,128)} %bitcast.26, s32[2,256]{1,0:T(2,128)} %bitcast.24, bf16[256,2048]{1,0:T(8,128)(2,1)} %rows_ref.1, f32[1,2048]{1,0:T(1,128)} %bitcast.23), custom_call_target="tpu_custom_call" | custom-call | tf_op jit(solution)/shard_map/dispatch/pallas_call | solution.py:269
  3.3 12.6 %all-to-all-start = ((bf16[32,32,128]{2,1,0:T(8,128)(2,1)}), bf16[32,32,128]{2,1,0:T(8,128)(2,1)S(1)}, u32[]{:S(2)}, u32[]{:S(2)}) async-start(bf16[32,32,128]{2,1,0:T(8,128)(2,1)} %get-tuple-element.14), calls=%async_computation | async-start | bytes 524288 | tf_op jit(solution)/shard_map/all_to_all | solution.py:283
  15.9 0.9 slice.9
  16.8 1.9 %prepare.1 = (bf16[2,256,1024]{2,1,0:T(8,128)(2,1)S(1)}, f32[2,256,128]{2,1,0:T(8,128)S(1)}, bf16[2048,256]{1,0:T(8,128)(2,1)S(1)}) custom-call(s32[2,256]{1,0:T(2,128)S(1)} %get-tuple-element.15.place_ref, f32[2,256]{1,0:T(2,128)} %bitcast.25, bf16[2048,128]{1,0:T(8,128)(2,1)} %bitcast.21, bf16[2048,128]{1,0:T(8,128)(2,1)} %bitcast.22), custom_call_target="tpu_custom_call" | custom-call | tf_op jit(solution)/shard_map/prepare/pallas_call | solution.py:284
  18.7 0.0 copy-start
  18.8 9.3 %all-to-all-done = bf16[32,32,128]{2,1,0:T(8,128)(2,1)S(1)} async-done(((bf16[32,32,128]{2,1,0:T(8,128)(2,1)}), bf16[32,32,128]{2,1,0:T(8,128)(2,1)S(1)}, u32[]{:S(2)}, u32[]{:S(2)}) %all-to-all-start) | async-done | bytes 262176 | tf_op jit(solution)/shard_map/all_to_all | solution.py:283
  28.1 0.1 convert_element_type.32
  28.1 0.1 convert_element_type.33
  28.3 0.0 copy-done
  28.3 32.3 %all-gather.3 = f16[1024,2048]{1,0:T(8,128)(2,1)S(1)} all-gather(f16[64,2048]{1,0:T(8,128)(2,1)S(1)} %convert_element_type.33), channel_id=1, replica_groups=mesh['ep'=32,'tp'=16] {'tp'}, dimensions={0}, use_global_device_ids=true | all-gather | bytes 4456448 | tf_op jit(solution)/shard_map/all_gather | solution.py:300
  60.6 1.2 %fusion.1.y_ref = f32[1024,256]{1,0:T(8,128)S(1)} fusion(bf16[2048,256]{1,0:T(8,128)(2,1)S(1)} %get-tuple-element.21, f16[1024,2048]{1,0:T(8,128)(2,1)S(1)} %all-gather.3), kind=kOutput, calls=%fused_computation.2 | convolution fusion | flops 1075838976 | bytes 6291456 | tf_op jit(solution)/shard_map/dot_general | solution.py:302
  61.8 0.6 hidden.1
  62.5 0.0 copy-start.4
  62.5 0.1 convert_element_type.35
  62.6 32.4 %all-gather.4 = f16[16640,128]{1,0:T(8,128)(2,1)S(1)} all-gather(f16[1040,128]{1,0:T(8,128)(2,1)S(1)} %convert_element_type.35), channel_id=2, replica_groups=mesh['ep'=32,'tp'=16] {'tp'}, dimensions={0}, use_global_device_ids=true | all-gather | bytes 4526080 | tf_op jit(solution)/shard_map/all_gather | solution.py:312
  95.0 0.2 fusion.8
  95.2 0.0 copy-done.4
  95.2 0.0 copy-start.2
  95.2 0.0 copy-start.3
  95.2 2.0 %fusion.4 = bf16[1024,128]{1,0:T(8,128)(2,1)} fusion(f16[16,1040,128]{2,1,0:T(8,128)(2,1)S(1)} %bitcast.20, bf16[16,128,128]{2,1,0:T(8,128)(2,1)S(1)} %bitcast.27, f32[16]{0:T(128)S(1)} %fusion.8), kind=kOutput, calls=%fused_computation.5 | convolution fusion | flops 539885568 | bytes 4981248 | tf_op jit(solution)/shard_map/trk,tko->ro/dot_general | solution.py:319
  97.2 5.1 %all-to-all-start.1 = ((bf16[32,32,128]{2,1,0:T(8,128)(2,1)}), bf16[32,32,128]{2,1,0:T(8,128)(2,1)S(1)}, u32[]{:S(2)}, u32[]{:S(2)}) async-start(bf16[32,32,128]{2,1,0:T(8,128)(2,1)} %bitcast.11), calls=%async_computation.1 | async-start | bytes 524288 | tf_op jit(solution)/shard_map/all_to_all | solution.py:325
  102.4 0.0 copy-start.1
  102.4 2.1 %collective-permute-start = (bf16[2,128,256]{2,1,0:T(8,128)(2,1)S(1)}, bf16[2,128,256]{2,1,0:T(8,128)(2,1)S(1)}, u32[]{:S(2)}, u32[]{:S(2)}) collective-permute-start(bf16[2,128,256]{2,1,0:T(8,128)(2,1)S(1)} %slice.9), channel_id=1, source_target_pairs={{0,1},{1,2},{2,3},{3,4},{4,5},{5,6},{6,7},{7,8},{8,9},{9,10},{10,1... | collective-permute-start | bytes 393224 | tf_op jit(solution)/shard_map/ppermute | solution.py:120
  104.5 0.0 copy-done.2
  104.5 0.0 copy-done.3
  104.5 4.3 %later_blocks.1.kept_ref = bf16[384,1024]{1,0:T(8,128)(2,1)} custom-call(f32[16]{0:T(128)} %sink_ref.1, bf16[384,1024]{1,0:T(8,128)(2,1)S(1)} %copy-done.3, bf16[2,384,256]{2,1,0:T(8,128)(2,1)S(1)} %copy-done.2), custom_call_target="tpu_custom_call" | custom-call | flops 2000000000 | bytes 2000000 | tf_op jit(solution)/shard_map/later_blocks/pallas_call | solution.py:141
  108.8 4.9 %collective-permute-done.edge_ref = bf16[2,128,256]{2,1,0:T(8,128)(2,1)S(1)} collective-permute-done((bf16[2,128,256]{2,1,0:T(8,128)(2,1)S(1)}, bf16[2,128,256]{2,1,0:T(8,128)(2,1)S(1)}, u32[]{:S(2)}, u32[]{:S(2)}) %collective-permute-start) | collective-permute-done | bytes 131104 | tf_op jit(solution)/shard_map/ppermute | solution.py:120
  113.7 3.0 %first_block.1 = bf16[384,1024]{1,0:T(8,128)(2,1)} custom-call(s32[1]{0:T(128)} %bitcast.first_ref, f32[16]{0:T(128)} %sink_ref.1, bf16[384,1024]{1,0:T(8,128)(2,1)S(1)} %copy-done.3, bf16[2,384,256]{2,1,0:T(8,128)(2,1)S(1)} %copy-done.2, bf16[2,128,256]{2,1,0:T(8,128)(2,1)S(1)} %collective-permute-done.edge_ref, ...), custom_call_target="tpu_custom_call", output_to_operand_aliasing={{}: (5, {})} | custom-call | flops 1000000000 | bytes 1000000 | tf_op jit(solution)/shard_map/first_block/pallas_call | solution.py:150
  116.6 0.0 all-to-all-done.1
  116.7 0.0 copy-done.1
  116.7 1.1 combine.1
Async XLA Ops:
  3.3 24.8 %all-to-all-start = ((bf16[32,32,128]{2,1,0:T(8,128)(2,1)}), bf16[32,32,128]{2,1,0:T(8,128)(2,1)S(1)}, u32[]{:S(2)}, u32[]{:S(2)}) async-start(bf16[32,32,128]{2,1,0:T(8,128)(2,1)} %get-tuple-element.14), calls=%async_computation | async-start | bytes 524288 | tf_op jit(solution)/shard_map/all_to_all | solution.py:283
  18.7 9.5 %copy-start = (f32[2,256,128]{2,1,0:T(8,128)}, f32[2,256,128]{2,1,0:T(8,128)S(1)}, u32[]{:S(2)}) copy-start(f32[2,256,128]{2,1,0:T(8,128)S(1)} %get-tuple-element.25.column_ref) | copy-start | bytes 786436
  62.5 32.7 %copy-start.4 = (bf16[1,2048,128]{2,1,0:T(8,128)(2,1)S(1)}, bf16[1,2048,128]{2,1,0:T(8,128)(2,1)}, u32[]{:S(2)}) copy-start(bf16[1,2048,128]{2,1,0:T(8,128)(2,1)} %param.21) | copy-start | bytes 1572868
  95.2 9.3 %copy-start.2 = (bf16[2,384,256]{2,1,0:T(8,128)(2,1)S(1)}, bf16[2,384,256]{2,1,0:T(8,128)(2,1)}, u32[]{:S(2)}) copy-start(bf16[2,384,256]{2,1,0:T(8,128)(2,1)} %kv_ref.3) | copy-start | bytes 1179652
  95.2 9.3 %copy-start.3 = (bf16[384,1024]{1,0:T(8,128)(2,1)S(1)}, bf16[384,1024]{1,0:T(8,128)(2,1)}, u32[]{:S(2)}) copy-start(bf16[384,1024]{1,0:T(8,128)(2,1)} %q_ref.3) | copy-start | bytes 2359300
  97.2 19.4 %all-to-all-start.1 = ((bf16[32,32,128]{2,1,0:T(8,128)(2,1)}), bf16[32,32,128]{2,1,0:T(8,128)(2,1)S(1)}, u32[]{:S(2)}, u32[]{:S(2)}) async-start(bf16[32,32,128]{2,1,0:T(8,128)(2,1)} %bitcast.11), calls=%async_computation.1 | async-start | bytes 524288 | tf_op jit(solution)/shard_map/all_to_all | solution.py:325
  102.4 14.3 %copy-start.1 = (f32[2,256,128]{2,1,0:T(8,128)S(1)}, f32[2,256,128]{2,1,0:T(8,128)}, u32[]{:S(2)}) copy-start(f32[2,256,128]{2,1,0:T(8,128)} %copy-done) | copy-start | bytes 786436
  102.4 11.3 %collective-permute-start = (bf16[2,128,256]{2,1,0:T(8,128)(2,1)S(1)}, bf16[2,128,256]{2,1,0:T(8,128)(2,1)S(1)}, u32[]{:S(2)}, u32[]{:S(2)}) collective-permute-start(bf16[2,128,256]{2,1,0:T(8,128)(2,1)S(1)} %slice.9), channel_id=1, source_target_pairs={{0,1},{1,2},{2,3},{3,4},{4,5},{5,6},{6,7},{7,8},{8,9},{9,10},{10,1... | collective-permute-start | bytes 393224 | tf_op jit(solution)/shard_map/ppermute | solution.py:120

commit v6 on v5

--- a/solution.py
+++ b/solution.py
@@ -50,6 +50,14 @@
                 band_ref[which, 2 * h, 1, at, :] = jnp.where(low, zero, turned)
                 band_ref[which, 2 * h + 1, 0, at, :] = jnp.where(low, turned, zero)
                 band_ref[which, 2 * h + 1, 1, at, :] = jnp.where(low, zero, value)
+
+    def written(block, c):
+        lanes = pl.ds(c * 256, 256)
+        return pltpu.make_async_copy(
+            done_ref.at[pl.ds(block * WINDOW, WINDOW), lanes],
+            out_ref.at[pl.ds((begin + block) * WINDOW, WINDOW), lanes],
+            copy_sem.at[block, c],
+        )
 
     if edge_ref is not None:
         absent = jnp.where(first_ref[0] == 1, f32(-1e30), f32(0.0))
@@ -96,11 +104,10 @@
                 done_ref[pl.ds(start, WINDOW), at : at + LANES] = (
                     summed[p * WINDOW : (p + 1) * WINDOW] / totals[p]
                 ).astype(bf16)
-    copy = pltpu.make_async_copy(
-        done_ref, out_ref.at[begin * WINDOW : (begin + blocks) * WINDOW, :], copy_sem
-    )
-    copy.start()
-    copy.wait()
+            written(block, c).start()
+    for block in range(blocks):
+        for c in range(KVH):
+            written(block, c).wait()
 
 
 def later_blocks_kernel(sink_ref, q_ref, kv_ref, out_ref, band_ref, done_ref, copy_sem):
@@ -134,7 +141,7 @@
         return [
             pltpu.VMEM((2, KVH, 2, (count + 1) * WINDOW, LANES), jnp.bfloat16),
             pltpu.VMEM((count * WINDOW, width), jnp.bfloat16),
-            pltpu.SemaphoreType.DMA,
+            pltpu.SemaphoreType.DMA((count, KVH)),
         ]
 
     result = jax.ShapeDtypeStruct(queries.shape, jnp.bfloat16)
@@ -159,23 +166,43 @@
     )(first, sink_logits, queries, keys_values, near(edge), later)
 
 
-def dispatch_kernel(mine_ref, group_ref, member_ref, rows_ref, gain_ref, out_ref, place_ref, normed_ref, line_ref):
+def dispatch_kernel(
+    mine_ref,
+    far_group_ref,
+    far_member_ref,
+    far_rows_ref,
+    far_gain_ref,
+    out_ref,
+    place_ref,
+    group_ref,
+    member_ref,
+    rows_ref,
+    gain_ref,
+    line_ref,
+    ready_ref,
+    sems,
+):
     f32 = jnp.float32
     bf16 = jnp.bfloat16
     tokens, width = rows_ref.shape
-    pieces = width // LANES
-    values = rows_ref[...].astype(f32)
-    mean = jnp.mean(values * values, axis=1, keepdims=True)
-    normed = (values * lax.rsqrt(mean + 1e-06) * gain_ref[...]).astype(bf16)
-    normed_ref[...] = normed * bf16(ROW_SCALE)
-    chosen = group_ref[...] * EPG + member_ref[...]
+    rows_copy = pltpu.make_async_copy(far_rows_ref, rows_ref, sems.at[0])
+    group_copy = pltpu.make_async_copy(far_group_ref, group_ref, sems.at[1])
+    member_copy = pltpu.make_async_copy(far_member_ref, member_ref, sems.at[2])
+    gain_copy = pltpu.make_async_copy(far_gain_ref, gain_ref, sems.at[3])
+    group_copy.start()
+    member_copy.start()
+    rows_copy.start()
+    gain_copy.start()
     which = lax.broadcasted_iota(jnp.int32, (EXPERTS, tokens), 0)
-    first = (which == chosen[0:1, :]).astype(f32)
-    second = (which == chosen[1:2, :]).astype(f32)
     before = (
         lax.broadcasted_iota(jnp.int32, (tokens, tokens), 0)
         < lax.broadcasted_iota(jnp.int32, (tokens, tokens), 1)
     ).astype(f32).astype(bf16)
+    group_copy.wait()
+    member_copy.wait()
+    chosen = group_ref[...] * EPG + member_ref[...]
+    first = (which == chosen[0:1, :]).astype(f32)
+    second = (which == chosen[1:2, :]).astype(f32)
     earlier = jnp.dot((first + second).astype(bf16), before, preferred_element_type=f32)
     places = []
     for k, hot in enumerate((first, second)):
@@ -187,10 +214,28 @@
     slot = lax.broadcasted_iota(jnp.int32, (slots, tokens), 0)
     wanted = (slot // share) * CAPACITY + mine_ref[0] * share + slot % share
     pick = ((places[0] == wanted) | (places[1] == wanted)).astype(f32).astype(bf16)
-    picked = jnp.dot(pick, normed_ref[...], preferred_element_type=f32)
+    rows_copy.wait()
+    gain_copy.wait()
+    values = jnp.dot(pick, rows_ref[...], preferred_element_type=f32)
+    mean = jnp.mean(values * values, axis=1, keepdims=True)
+    normed = (values * lax.rsqrt(mean + 1e-06) * gain_ref[...]).astype(bf16).astype(f32) * ROW_SCALE
+    pieces = width // LANES
     for j in range(pieces):
-        line_ref[pl.ds(j, slots, stride=pieces), :] = picked[:, j * LANES : (j + 1) * LANES]
-    out_ref[...] = line_ref[...].reshape(out_ref.shape).astype(bf16)
+        line_ref[pl.ds(j, slots, stride=pieces), :] = normed[:, j * LANES : (j + 1) * LANES]
+    half = EXPERTS // 2
+    rows = share * pieces
+    copies = []
+    for i in range(2):
+        part = line_ref[i * half * rows : (i + 1) * half * rows, :].reshape(half, rows, LANES)
+        ready_ref[i * half : (i + 1) * half] = part.astype(bf16)
+        copies.append(
+            pltpu.make_async_copy(
+                ready_ref.at[pl.ds(i * half, half)], out_ref.at[pl.ds(i * half, half)], sems.at[4 + i]
+            )
+        )
+        copies[i].start()
+    for copy in copies:
+        copy.wait()
 
 
 def prepare_kernel(
@@ -268,15 +313,20 @@
     outside = pl.BlockSpec(memory_space=pl.ANY)
     outgoing, places = pl.pallas_call(
         dispatch_kernel,
-        in_specs=[scalar, whole, whole, whole, whole],
-        out_specs=[whole, whole],
+        in_specs=[scalar, outside, outside, outside, outside],
+        out_specs=[outside, whole],
         out_shape=[
             jax.ShapeDtypeStruct((EXPERTS, share * width // LANES, LANES), bf16),
             pltpu.VMEM((TOP, tokens), jnp.int32),
         ],
         scratch_shapes=[
+            pltpu.VMEM((1, tokens), jnp.int32),
+            pltpu.VMEM((TOP, tokens), jnp.int32),
             pltpu.VMEM((tokens, width), bf16),
+            pltpu.VMEM((1, width), jnp.float32),
             pltpu.VMEM((slots * width // LANES, LANES), jnp.float32),
+            pltpu.VMEM((EXPERTS, share * width // LANES, LANES), bf16),
+            pltpu.SemaphoreType.DMA((6,)),
         ],
         name="dispatch",
     )(mine, group_choice[None, :], member_choice.T, moe_rows, norm_gain[None, :])

time: 118 us -> 118 us (level)
  no operation moved by 1% of the time
where the time goes in v6:
time: 118 us
  blocking collectives  64.7 us (55%)
  starting transfers between devices  19.8 us (17%)
  waiting for transfers between devices  14.3 us (12%)
  Pallas kernels  13.3 us (11%)
  matrix products  3.28 us (3%)
    all_gather x1, blocking collectives, route_experts(): lax.all_gather(hidden.astype(jnp.float16), 'tp', axis=0, tiled=False)  32.4 us
    all_gather x1, blocking collectives, route_experts(): block_rows = lax.all_gather(shared, 'tp', axis=0, tiled=True).astype(bf16)  32.3 us
    all_to_all x1, starting transfers between devices, route_experts(): incoming = lax.all_to_all(outgoing, 'ep', 0, 0, tiled=True)  12.6 us
    all_to_all x1, waiting for transfers between devices, route_experts(): incoming = lax.all_to_all(outgoing, 'ep', 0, 0, tiled=True)  9.32 us
    all_to_all x1, starting transfers between devices, route_experts(): lax.all_to_all(produced.reshape(total // CAPACITY, CAPACITY, out_width),...  5.15 us
    ppermute x1, waiting for transfers between devices, passed_along(): return lax.ppermute(value, ('ep', 'tp'), pairs)  4.99 us
    pallas_call x1, Pallas kernels, attend_window(): pl.pallas_call(later_blocks_kernel, in_specs=[scalar, whole, whole], out_...  4.2 us
    pallas_call x1, Pallas kernels, attend_window(): pl.pallas_call(first_block_kernel, in_specs=[scalar, scalar, whole, whole...  2.92 us
  transfers between devices with their start and end apart: 3, of which 2 were waited for; matrix products, arithmetic and copies ran while one was open for 1% of the time, Pallas kernels for 8%

profile of v6, /device:TPU:64, one launch (start us, length us, event | category | flops | bytes accessed | tf_op | source)
XLA Modules:
  0.0 117.6 jit_solution(7546924190963584423)
XLA Ops:
  0.6 2.6 %dispatch.1 = (bf16[32,32,128]{2,1,0:T(8,128)(2,1)}, s32[2,256]{1,0:T(2,128)S(1)}) custom-call(s32[1]{0:T(128)} %bitcast.1.mine_ref, s32[1,256]{1,0:T(1,128)} %bitcast.26, s32[2,256]{1,0:T(2,128)} %bitcast.24, bf16[256,2048]{1,0:T(8,128)(2,1)} %far_rows_ref.1, f32[1,2048]{1,0:T(1,128)} %bitcast.23), custom_call_target="tpu_custom_call" | custom-call | tf_op jit(solution)/shard_map/dispatch/pallas_call | solution.py:314
  3.2 12.6 %all-to-all-start = ((bf16[32,32,128]{2,1,0:T(8,128)(2,1)}), bf16[32,32,128]{2,1,0:T(8,128)(2,1)S(1)}, u32[]{:S(2)}, u32[]{:S(2)}) async-start(bf16[32,32,128]{2,1,0:T(8,128)(2,1)} %get-tuple-element.14), calls=%async_computation | async-start | bytes 524288 | tf_op jit(solution)/shard_map/all_to_all | solution.py:333
  15.9 0.9 slice.9
  16.8 1.9 %prepare.1 = (bf16[2,256,1024]{2,1,0:T(8,128)(2,1)S(1)}, f32[2,256,128]{2,1,0:T(8,128)S(1)}, bf16[2048,256]{1,0:T(8,128)(2,1)S(1)}) custom-call(s32[2,256]{1,0:T(2,128)S(1)} %get-tuple-element.15.place_ref, f32[2,256]{1,0:T(2,128)} %bitcast.25, bf16[2048,128]{1,0:T(8,128)(2,1)} %bitcast.21, bf16[2048,128]{1,0:T(8,128)(2,1)} %bitcast.22), custom_call_target="tpu_custom_call" | custom-call | tf_op jit(solution)/shard_map/prepare/pallas_call | solution.py:334
  18.7 0.0 copy-start
  18.7 9.3 %all-to-all-done = bf16[32,32,128]{2,1,0:T(8,128)(2,1)S(1)} async-done(((bf16[32,32,128]{2,1,0:T(8,128)(2,1)}), bf16[32,32,128]{2,1,0:T(8,128)(2,1)S(1)}, u32[]{:S(2)}, u32[]{:S(2)}) %all-to-all-start) | async-done | bytes 262176 | tf_op jit(solution)/shard_map/all_to_all | solution.py:333
  28.0 0.1 convert_element_type.32
  28.1 0.1 convert_element_type.33
  28.2 0.0 copy-done
  28.2 32.3 %all-gather.3 = f16[1024,2048]{1,0:T(8,128)(2,1)S(1)} all-gather(f16[64,2048]{1,0:T(8,128)(2,1)S(1)} %convert_element_type.33), channel_id=1, replica_groups=mesh['ep'=32,'tp'=16] {'tp'}, dimensions={0}, use_global_device_ids=true | all-gather | bytes 4456448 | tf_op jit(solution)/shard_map/all_gather | solution.py:350
  60.5 1.2 %fusion.1.y_ref = f32[1024,256]{1,0:T(8,128)S(1)} fusion(bf16[2048,256]{1,0:T(8,128)(2,1)S(1)} %get-tuple-element.21, f16[1024,2048]{1,0:T(8,128)(2,1)S(1)} %all-gather.3), kind=kOutput, calls=%fused_computation.2 | convolution fusion | flops 1075838976 | bytes 6291456 | tf_op jit(solution)/shard_map/dot_general | solution.py:352
  61.8 0.6 hidden.1
  62.4 0.0 copy-start.4
  62.5 0.1 convert_element_type.35
  62.5 32.4 %all-gather.4 = f16[16640,128]{1,0:T(8,128)(2,1)S(1)} all-gather(f16[1040,128]{1,0:T(8,128)(2,1)S(1)} %convert_element_type.35), channel_id=2, replica_groups=mesh['ep'=32,'tp'=16] {'tp'}, dimensions={0}, use_global_device_ids=true | all-gather | bytes 4526080 | tf_op jit(solution)/shard_map/all_gather | solution.py:362
  94.9 0.2 fusion.8
  95.1 0.0 copy-done.4
  95.1 0.0 copy-start.2
  95.2 0.0 copy-start.3
  95.2 2.0 %fusion.4 = bf16[1024,128]{1,0:T(8,128)(2,1)} fusion(f16[16,1040,128]{2,1,0:T(8,128)(2,1)S(1)} %bitcast.20, bf16[16,128,128]{2,1,0:T(8,128)(2,1)S(1)} %bitcast.27, f32[16]{0:T(128)S(1)} %fusion.8), kind=kOutput, calls=%fused_computation.5 | convolution fusion | flops 539885568 | bytes 4981248 | tf_op jit(solution)/shard_map/trk,tko->ro/dot_general | solution.py:369
  97.2 5.1 %all-to-all-start.1 = ((bf16[32,32,128]{2,1,0:T(8,128)(2,1)}), bf16[32,32,128]{2,1,0:T(8,128)(2,1)S(1)}, u32[]{:S(2)}, u32[]{:S(2)}) async-start(bf16[32,32,128]{2,1,0:T(8,128)(2,1)} %bitcast.11), calls=%async_computation.1 | async-start | bytes 524288 | tf_op jit(solution)/shard_map/all_to_all | solution.py:375
  102.4 0.0 copy-start.1
  102.4 2.1 %collective-permute-start = (bf16[2,128,256]{2,1,0:T(8,128)(2,1)S(1)}, bf16[2,128,256]{2,1,0:T(8,128)(2,1)S(1)}, u32[]{:S(2)}, u32[]{:S(2)}) collective-permute-start(bf16[2,128,256]{2,1,0:T(8,128)(2,1)S(1)} %slice.9), channel_id=1, source_target_pairs={{0,1},{1,2},{2,3},{3,4},{4,5},{5,6},{6,7},{7,8},{8,9},{9,10},{10,1... | collective-permute-start | bytes 393224 | tf_op jit(solution)/shard_map/ppermute | solution.py:127
  104.4 0.0 copy-done.2
  104.4 0.0 copy-done.3
  104.4 4.2 %later_blocks.1.kept_ref = bf16[384,1024]{1,0:T(8,128)(2,1)} custom-call(f32[16]{0:T(128)} %sink_ref.1, bf16[384,1024]{1,0:T(8,128)(2,1)S(1)} %copy-done.3, bf16[2,384,256]{2,1,0:T(8,128)(2,1)S(1)} %copy-done.2), custom_call_target="tpu_custom_call" | custom-call | flops 2000000000 | bytes 2000000 | tf_op jit(solution)/shard_map/later_blocks/pallas_call | solution.py:148
  108.7 5.0 %collective-permute-done.edge_ref = bf16[2,128,256]{2,1,0:T(8,128)(2,1)S(1)} collective-permute-done((bf16[2,128,256]{2,1,0:T(8,128)(2,1)S(1)}, bf16[2,128,256]{2,1,0:T(8,128)(2,1)S(1)}, u32[]{:S(2)}, u32[]{:S(2)}) %collective-permute-start) | collective-permute-done | bytes 131104 | tf_op jit(solution)/shard_map/ppermute | solution.py:127
  113.6 2.9 %first_block.1 = bf16[384,1024]{1,0:T(8,128)(2,1)} custom-call(s32[1]{0:T(128)} %bitcast.first_ref, f32[16]{0:T(128)} %sink_ref.1, bf16[384,1024]{1,0:T(8,128)(2,1)S(1)} %copy-done.3, bf16[2,384,256]{2,1,0:T(8,128)(2,1)S(1)} %copy-done.2, bf16[2,128,256]{2,1,0:T(8,128)(2,1)S(1)} %collective-permute-done.edge_ref, ...), custom_call_target="tpu_custom_call", output_to_operand_aliasing={{}: (5, {})} | custom-call | flops 1000000000 | bytes 1000000 | tf_op jit(solution)/shard_map/first_block/pallas_call | solution.py:157
  116.6 0.0 all-to-all-done.1
  116.6 0.0 copy-done.1
  116.6 1.1 combine.1
Async XLA Ops:
  3.2 24.8 %all-to-all-start = ((bf16[32,32,128]{2,1,0:T(8,128)(2,1)}), bf16[32,32,128]{2,1,0:T(8,128)(2,1)S(1)}, u32[]{:S(2)}, u32[]{:S(2)}) async-start(bf16[32,32,128]{2,1,0:T(8,128)(2,1)} %get-tuple-element.14), calls=%async_computation | async-start | bytes 524288 | tf_op jit(solution)/shard_map/all_to_all | solution.py:333
  18.7 9.5 %copy-start = (f32[2,256,128]{2,1,0:T(8,128)}, f32[2,256,128]{2,1,0:T(8,128)S(1)}, u32[]{:S(2)}) copy-start(f32[2,256,128]{2,1,0:T(8,128)S(1)} %get-tuple-element.25.column_ref) | copy-start | bytes 786436
  62.4 32.7 %copy-start.4 = (bf16[1,2048,128]{2,1,0:T(8,128)(2,1)S(1)}, bf16[1,2048,128]{2,1,0:T(8,128)(2,1)}, u32[]{:S(2)}) copy-start(bf16[1,2048,128]{2,1,0:T(8,128)(2,1)} %param.21) | copy-start | bytes 1572868
  95.1 9.3 %copy-start.2 = (bf16[2,384,256]{2,1,0:T(8,128)(2,1)S(1)}, bf16[2,384,256]{2,1,0:T(8,128)(2,1)}, u32[]{:S(2)}) copy-start(bf16[2,384,256]{2,1,0:T(8,128)(2,1)} %kv_ref.3) | copy-start | bytes 1179652
  95.2 9.3 %copy-start.3 = (bf16[384,1024]{1,0:T(8,128)(2,1)S(1)}, bf16[384,1024]{1,0:T(8,128)(2,1)}, u32[]{:S(2)}) copy-start(bf16[384,1024]{1,0:T(8,128)(2,1)} %q_ref.3) | copy-start | bytes 2359300
  97.2 19.4 %all-to-all-start.1 = ((bf16[32,32,128]{2,1,0:T(8,128)(2,1)}), bf16[32,32,128]{2,1,0:T(8,128)(2,1)S(1)}, u32[]{:S(2)}, u32[]{:S(2)}) async-start(bf16[32,32,128]{2,1,0:T(8,128)(2,1)} %bitcast.11), calls=%async_computation.1 | async-start | bytes 524288 | tf_op jit(solution)/shard_map/all_to_all | solution.py:375
  102.4 14.2 %copy-start.1 = (f32[2,256,128]{2,1,0:T(8,128)S(1)}, f32[2,256,128]{2,1,0:T(8,128)}, u32[]{:S(2)}) copy-start(f32[2,256,128]{2,1,0:T(8,128)} %copy-done) | copy-start | bytes 786436
  102.4 11.3 %collective-permute-start = (bf16[2,128,256]{2,1,0:T(8,128)(2,1)S(1)}, bf16[2,128,256]{2,1,0:T(8,128)(2,1)S(1)}, u32[]{:S(2)}, u32[]{:S(2)}) collective-permute-start(bf16[2,128,256]{2,1,0:T(8,128)(2,1)S(1)} %slice.9), channel_id=1, source_target_pairs={{0,1},{1,2},{2,3},{3,4},{4,5},{5,6},{6,7},{7,8},{8,9},{9,10},{10,1... | collective-permute-start | bytes 393224 | tf_op jit(solution)/shard_map/ppermute | solution.py:127

commit v7 on v6

--- a/solution.py
+++ b/solution.py
@@ -24,7 +24,7 @@
 
 
 def attend_blocks(
-    begin, blocks, first_ref, sink_ref, q_ref, kv_ref, edge_ref, out_ref, band_ref, done_ref, copy_sem
+    begin, blocks, first_ref, sink_ref, q_ref, kv_ref, edge_ref, shared_ref, out_ref, band_ref, done_ref, copy_sem
 ):
     f32 = jnp.float32
     bf16 = jnp.bfloat16
@@ -33,8 +33,12 @@
     causal = col <= row
     low = lax.broadcasted_iota(jnp.int32, (WINDOW, LANES), 1) < HD
     zero = jnp.zeros((WINDOW, LANES), bf16)
+    parts = blocks + 1
+    if edge_ref is not None:
+        parts = 1
+        band_ref[:, :, :, WINDOW : 2 * WINDOW, :] = shared_ref[...]
     for which in range(2):
-        for part in range(blocks + 1):
+        for part in range(parts):
             for h in range(KVH // 2):
                 lanes = slice(h * LANES, (h + 1) * LANES)
                 if part == 0 and edge_ref is not None:
@@ -50,6 +54,9 @@
                 band_ref[which, 2 * h, 1, at, :] = jnp.where(low, zero, turned)
                 band_ref[which, 2 * h + 1, 0, at, :] = jnp.where(low, turned, zero)
                 band_ref[which, 2 * h + 1, 1, at, :] = jnp.where(low, zero, value)
+
+    if edge_ref is None:
+        shared_ref[...] = band_ref[:, :, :, :WINDOW, :]
 
     def written(block, c):
         lanes = pl.ds(c * 256, 256)
@@ -110,15 +117,19 @@
             written(block, c).wait()
 
 
-def later_blocks_kernel(sink_ref, q_ref, kv_ref, out_ref, band_ref, done_ref, copy_sem):
+def later_blocks_kernel(sink_ref, q_ref, kv_ref, out_ref, shared_ref, band_ref, done_ref, copy_sem):
     blocks = q_ref.shape[0] // WINDOW - 1
-    attend_blocks(1, blocks, None, sink_ref, q_ref, kv_ref, None, out_ref, band_ref, done_ref, copy_sem)
+    attend_blocks(
+        1, blocks, None, sink_ref, q_ref, kv_ref, None, shared_ref, out_ref, band_ref, done_ref, copy_sem
+    )
 
 
 def first_block_kernel(
-    first_ref, sink_ref, q_ref, kv_ref, edge_ref, kept_ref, out_ref, band_ref, done_ref, copy_sem
-):
-    attend_blocks(0, 1, first_ref, sink_ref, q_ref, kv_ref, edge_ref, out_ref, band_ref, done_ref, copy_sem)
+    first_ref, sink_ref, q_ref, shared_ref, edge_ref, kept_ref, out_ref, band_ref, done_ref, copy_sem
+):
+    attend_blocks(
+        0, 1, first_ref, sink_ref, q_ref, None, edge_ref, shared_ref, out_ref, band_ref, done_ref, copy_sem
+    )
 
 
 def passed_along(value):
@@ -145,11 +156,11 @@
         ]
 
     result = jax.ShapeDtypeStruct(queries.shape, jnp.bfloat16)
-    later = pl.pallas_call(
+    later, shared = pl.pallas_call(
         later_blocks_kernel,
         in_specs=[scalar, whole, whole],
-        out_specs=outside,
-        out_shape=result,
+        out_specs=[outside, whole],
+        out_shape=[result, pltpu.VMEM((2, KVH, 2, WINDOW, LANES), jnp.bfloat16)],
         scratch_shapes=scratch(blocks - 1),
         cost_estimate=pl.CostEstimate(flops=2 * 10**9, bytes_accessed=2 * 10**6, transcendentals=10**6),
         name="later_blocks",
@@ -163,7 +174,7 @@
         input_output_aliases={5: 0},
         cost_estimate=pl.CostEstimate(flops=10**9, bytes_accessed=10**6, transcendentals=10**6),
         name="first_block",
-    )(first, sink_logits, queries, keys_values, near(edge), later)
+    )(first, sink_logits, queries, near(shared), near(edge), later)
 
 
 def dispatch_kernel(
@@ -292,11 +303,12 @@
 
 
 def combine_kernel(hot_ref, column_ref, rows_ref, out_ref):
-    total = None
-    for k in range(TOP):
-        picked = jnp.dot(hot_ref[k], rows_ref[...], preferred_element_type=jnp.float32)
-        part = column_ref[k] * picked
-        total = part if total is None else total + part
+    picks, tokens, slots = hot_ref.shape
+    hot = hot_ref[...].reshape(picks * tokens, slots)
+    picked = jnp.dot(hot, rows_ref[...], preferred_element_type=jnp.float32)
+    total = column_ref[0] * picked[:tokens]
+    for k in range(1, picks):
+        total = total + column_ref[k] * picked[k * tokens : (k + 1) * tokens]
     out_ref[...] = total.astype(jnp.bfloat16)
 
 

time: 118 us -> 118 us (level)
  no operation moved by 1% of the time
where the time goes in v7:
time: 118 us
  blocking collectives  64.7 us (55%)
  starting transfers between devices  19.8 us (17%)
  waiting for transfers between devices  14.3 us (12%)
  Pallas kernels  13.4 us (11%)
  matrix products  3.29 us (3%)
    all_gather x1, blocking collectives, route_experts(): lax.all_gather(hidden.astype(jnp.float16), 'tp', axis=0, tiled=False)  32.4 us
    all_gather x1, blocking collectives, route_experts(): block_rows = lax.all_gather(shared, 'tp', axis=0, tiled=True).astype(bf16)  32.3 us
    all_to_all x1, starting transfers between devices, route_experts(): incoming = lax.all_to_all(outgoing, 'ep', 0, 0, tiled=True)  12.6 us
    all_to_all x1, waiting for transfers between devices, route_experts(): incoming = lax.all_to_all(outgoing, 'ep', 0, 0, tiled=True)  9.32 us
    all_to_all x1, starting transfers between devices, route_experts(): lax.all_to_all(produced.reshape(total // CAPACITY, CAPACITY, out_width),...  5.14 us
    ppermute x1, waiting for transfers between devices, passed_along(): return lax.ppermute(value, ('ep', 'tp'), pairs)  4.95 us
    pallas_call x1, Pallas kernels, attend_window(): pl.pallas_call(later_blocks_kernel, in_specs=[scalar, whole, whole], out_...  4.24 us
    pallas_call x1, Pallas kernels, attend_window(): pl.pallas_call(first_block_kernel, in_specs=[scalar, scalar, whole, whole...  2.93 us
  transfers between devices with their start and end apart: 3, of which 2 were waited for; matrix products, arithmetic and copies ran while one was open for 1% of the time, Pallas kernels for 8%

profile of v7, /device:TPU:64, one launch (start us, length us, event | category | flops | bytes accessed | tf_op | source)
XLA Modules:
  0.0 117.7 jit_solution(11259184394686983636)
XLA Ops:
  0.6 2.6 %dispatch.1 = (bf16[32,32,128]{2,1,0:T(8,128)(2,1)}, s32[2,256]{1,0:T(2,128)S(1)}) custom-call(s32[1]{0:T(128)} %bitcast.1.mine_ref, s32[1,256]{1,0:T(1,128)} %bitcast.26, s32[2,256]{1,0:T(2,128)} %bitcast.24, bf16[256,2048]{1,0:T(8,128)(2,1)} %far_rows_ref.1, f32[1,2048]{1,0:T(1,128)} %bitcast.23), custom_call_target="tpu_custom_call" | custom-call | tf_op jit(solution)/shard_map/dispatch/pallas_call | solution.py:326
  3.2 12.6 %all-to-all-start = ((bf16[32,32,128]{2,1,0:T(8,128)(2,1)}), bf16[32,32,128]{2,1,0:T(8,128)(2,1)S(1)}, u32[]{:S(2)}, u32[]{:S(2)}) async-start(bf16[32,32,128]{2,1,0:T(8,128)(2,1)} %get-tuple-element.16), calls=%async_computation | async-start | bytes 524288 | tf_op jit(solution)/shard_map/all_to_all | solution.py:345
  15.9 0.9 slice.9
  16.8 1.9 %prepare.1 = (bf16[2,256,1024]{2,1,0:T(8,128)(2,1)S(1)}, f32[2,256,128]{2,1,0:T(8,128)S(1)}, bf16[2048,256]{1,0:T(8,128)(2,1)S(1)}) custom-call(s32[2,256]{1,0:T(2,128)S(1)} %get-tuple-element.17.place_ref, f32[2,256]{1,0:T(2,128)} %bitcast.25, bf16[2048,128]{1,0:T(8,128)(2,1)} %bitcast.21, bf16[2048,128]{1,0:T(8,128)(2,1)} %bitcast.22), custom_call_target="tpu_custom_call" | custom-call | tf_op jit(solution)/shard_map/prepare/pallas_call | solution.py:346
  18.7 0.0 copy-start
  18.7 9.3 %all-to-all-done = bf16[32,32,128]{2,1,0:T(8,128)(2,1)S(1)} async-done(((bf16[32,32,128]{2,1,0:T(8,128)(2,1)}), bf16[32,32,128]{2,1,0:T(8,128)(2,1)S(1)}, u32[]{:S(2)}, u32[]{:S(2)}) %all-to-all-start) | async-done | bytes 262176 | tf_op jit(solution)/shard_map/all_to_all | solution.py:345
  28.0 0.1 convert_element_type.32
  28.1 0.1 convert_element_type.33
  28.2 0.0 copy-done
  28.2 32.3 %all-gather.3 = f16[1024,2048]{1,0:T(8,128)(2,1)S(1)} all-gather(f16[64,2048]{1,0:T(8,128)(2,1)S(1)} %convert_element_type.33), channel_id=1, replica_groups=mesh['ep'=32,'tp'=16] {'tp'}, dimensions={0}, use_global_device_ids=true | all-gather | bytes 4456448 | tf_op jit(solution)/shard_map/all_gather | solution.py:362
  60.5 1.2 %fusion.1.y_ref = f32[1024,256]{1,0:T(8,128)S(1)} fusion(bf16[2048,256]{1,0:T(8,128)(2,1)S(1)} %get-tuple-element.23, f16[1024,2048]{1,0:T(8,128)(2,1)S(1)} %all-gather.3), kind=kOutput, calls=%fused_computation.2 | convolution fusion | flops 1075838976 | bytes 6291456 | tf_op jit(solution)/shard_map/dot_general | solution.py:364
  61.8 0.6 hidden.1
  62.4 0.0 copy-start.4
  62.5 0.1 convert_element_type.35
  62.5 32.4 %all-gather.4 = f16[16640,128]{1,0:T(8,128)(2,1)S(1)} all-gather(f16[1040,128]{1,0:T(8,128)(2,1)S(1)} %convert_element_type.35), channel_id=2, replica_groups=mesh['ep'=32,'tp'=16] {'tp'}, dimensions={0}, use_global_device_ids=true | all-gather | bytes 4526080 | tf_op jit(solution)/shard_map/all_gather | solution.py:374
  94.9 0.2 fusion.8
  95.1 0.0 copy-done.4
  95.1 0.0 copy-start.2
  95.2 0.0 copy-start.3
  95.2 2.0 %fusion.4 = bf16[1024,128]{1,0:T(8,128)(2,1)} fusion(f16[16,1040,128]{2,1,0:T(8,128)(2,1)S(1)} %bitcast.20, bf16[16,128,128]{2,1,0:T(8,128)(2,1)S(1)} %bitcast.27, f32[16]{0:T(128)S(1)} %fusion.8), kind=kOutput, calls=%fused_computation.5 | convolution fusion | flops 539885568 | bytes 4981248 | tf_op jit(solution)/shard_map/trk,tko->ro/dot_general | solution.py:381
  97.2 5.1 %all-to-all-start.1 = ((bf16[32,32,128]{2,1,0:T(8,128)(2,1)}), bf16[32,32,128]{2,1,0:T(8,128)(2,1)S(1)}, u32[]{:S(2)}, u32[]{:S(2)}) async-start(bf16[32,32,128]{2,1,0:T(8,128)(2,1)} %bitcast.11), calls=%async_computation.1 | async-start | bytes 524288 | tf_op jit(solution)/shard_map/all_to_all | solution.py:387
  102.4 0.0 copy-start.1
  102.4 2.1 %collective-permute-start = (bf16[2,128,256]{2,1,0:T(8,128)(2,1)S(1)}, bf16[2,128,256]{2,1,0:T(8,128)(2,1)S(1)}, u32[]{:S(2)}, u32[]{:S(2)}) collective-permute-start(bf16[2,128,256]{2,1,0:T(8,128)(2,1)S(1)} %slice.9), channel_id=1, source_target_pairs={{0,1},{1,2},{2,3},{3,4},{4,5},{5,6},{6,7},{7,8},{8,9},{9,10},{10,1... | collective-permute-start | bytes 393224 | tf_op jit(solution)/shard_map/ppermute | solution.py:138
  104.4 0.0 copy-done.2
  104.4 0.0 copy-done.3
  104.5 4.2 %later_blocks.1 = (bf16[384,1024]{1,0:T(8,128)(2,1)}, bf16[2,4,2,128,128]{4,3,2,1,0:T(8,128)(2,1)S(1)}) custom-call(f32[16]{0:T(128)} %sink_ref.1, bf16[384,1024]{1,0:T(8,128)(2,1)S(1)} %copy-done.3, bf16[2,384,256]{2,1,0:T(8,128)(2,1)S(1)} %copy-done.2), custom_call_target="tpu_custom_call" | custom-call | flops 2000000000 | bytes 2000000 | tf_op jit(solution)/shard_map/later_blocks/pallas_call | solution.py:159
  108.7 5.0 %collective-permute-done.edge_ref = bf16[2,128,256]{2,1,0:T(8,128)(2,1)S(1)} collective-permute-done((bf16[2,128,256]{2,1,0:T(8,128)(2,1)S(1)}, bf16[2,128,256]{2,1,0:T(8,128)(2,1)S(1)}, u32[]{:S(2)}, u32[]{:S(2)}) %collective-permute-start) | collective-permute-done | bytes 131104 | tf_op jit(solution)/shard_map/ppermute | solution.py:138
  113.6 2.9 %first_block.1 = bf16[384,1024]{1,0:T(8,128)(2,1)} custom-call(s32[1]{0:T(128)} %bitcast.first_ref, f32[16]{0:T(128)} %sink_ref.1, bf16[384,1024]{1,0:T(8,128)(2,1)S(1)} %copy-done.3, bf16[2,4,2,128,128]{4,3,2,1,0:T(8,128)(2,1)S(1)} %get-tuple-element.25.shared_ref, ...), custom_call_target="tpu_custom_call", output_to_operand_aliasing={{}: (5, {})} | custom-call | flops 1000000000 | bytes 1000000 | tf_op jit(solution)/shard_map/first_block/pallas_call | solution.py:168
  116.6 0.0 all-to-all-done.1
  116.6 0.0 copy-done.1
  116.6 1.1 combine.1
Async XLA Ops:
  3.2 24.8 %all-to-all-start = ((bf16[32,32,128]{2,1,0:T(8,128)(2,1)}), bf16[32,32,128]{2,1,0:T(8,128)(2,1)S(1)}, u32[]{:S(2)}, u32[]{:S(2)}) async-start(bf16[32,32,128]{2,1,0:T(8,128)(2,1)} %get-tuple-element.16), calls=%async_computation | async-start | bytes 524288 | tf_op jit(solution)/shard_map/all_to_all | solution.py:345
  18.7 9.5 %copy-start = (f32[2,256,128]{2,1,0:T(8,128)}, f32[2,256,128]{2,1,0:T(8,128)S(1)}, u32[]{:S(2)}) copy-start(f32[2,256,128]{2,1,0:T(8,128)S(1)} %get-tuple-element.29.column_ref) | copy-start | bytes 786436
  62.4 32.7 %copy-start.4 = (bf16[1,2048,128]{2,1,0:T(8,128)(2,1)S(1)}, bf16[1,2048,128]{2,1,0:T(8,128)(2,1)}, u32[]{:S(2)}) copy-start(bf16[1,2048,128]{2,1,0:T(8,128)(2,1)} %param.21) | copy-start | bytes 1572868
  95.1 9.3 %copy-start.2 = (bf16[2,384,256]{2,1,0:T(8,128)(2,1)S(1)}, bf16[2,384,256]{2,1,0:T(8,128)(2,1)}, u32[]{:S(2)}) copy-start(bf16[2,384,256]{2,1,0:T(8,128)(2,1)} %kv_ref.1) | copy-start | bytes 1179652
  95.2 9.3 %copy-start.3 = (bf16[384,1024]{1,0:T(8,128)(2,1)S(1)}, bf16[384,1024]{1,0:T(8,128)(2,1)}, u32[]{:S(2)}) copy-start(bf16[384,1024]{1,0:T(8,128)(2,1)} %q_ref.3) | copy-start | bytes 2359300
  97.2 19.4 %all-to-all-start.1 = ((bf16[32,32,128]{2,1,0:T(8,128)(2,1)}), bf16[32,32,128]{2,1,0:T(8,128)(2,1)S(1)}, u32[]{:S(2)}, u32[]{:S(2)}) async-start(bf16[32,32,128]{2,1,0:T(8,128)(2,1)} %bitcast.11), calls=%async_computation.1 | async-start | bytes 524288 | tf_op jit(solution)/shard_map/all_to_all | solution.py:387
  102.4 14.2 %copy-start.1 = (f32[2,256,128]{2,1,0:T(8,128)S(1)}, f32[2,256,128]{2,1,0:T(8,128)}, u32[]{:S(2)}) copy-start(f32[2,256,128]{2,1,0:T(8,128)} %copy-done) | copy-start | bytes 786436
  102.4 11.3 %collective-permute-start = (bf16[2,128,256]{2,1,0:T(8,128)(2,1)S(1)}, bf16[2,128,256]{2,1,0:T(8,128)(2,1)S(1)}, u32[]{:S(2)}, u32[]{:S(2)}) collective-permute-start(bf16[2,128,256]{2,1,0:T(8,128)(2,1)S(1)} %slice.9), channel_id=1, source_target_pairs={{0,1},{1,2},{2,3},{3,4},{4,5},{5,6},{6,7},{7,8},{8,9},{9,10},{10,1... | collective-permute-start | bytes 393224 | tf_op jit(solution)/shard_map/ppermute | solution.py:138
